TPU v7x, 256 devices: a whole 4x4x8 slice. The times are simulated.
256 devices in a mesh: sp: 64 (over z, x, core), tp: 4 (over y).
Axes of the slice: x: 4, y: 4, z: 8, core: 2. Of those that a mesh axis runs over, the one named last changes fastest.
Arguments:
- residual: bfloat16 [16384, 2048], P(('sp', 'tp')), may hold values from -6 to 6
- query_wide: bfloat16 [16384, 512], P('sp', 'tp'), may hold values from -8 to 8
- key_wide: bfloat16 [16384, 512], P('sp', 'tp'), may hold values from -8 to 8
- value_wide: bfloat16 [16384, 512], P('sp', 'tp'), may hold values from -6 to 6
- query_narrow: bfloat16 [16384, 512], P('sp', 'tp'), may hold values from -8 to 8
- key_narrow: bfloat16 [16384, 512], P('sp', 'tp'), may hold values from -8 to 8
- value_narrow: bfloat16 [16384, 512], P('sp', 'tp'), may hold values from -6 to 6
- gate_wide: float32 [16384, 4], P('sp', 'tp'), may hold values from -2 to 20
- gate_narrow: float32 [16384, 8], P('sp', 'tp'), may hold values from -2 to 20
- out_wide: bfloat16 [512, 2048], replicated, may hold values from -0.1875 to 0.1875
- out_narrow: bfloat16 [512, 2048], replicated, may hold values from -0.1875 to 0.1875
- norm_gain: float32 [2048], replicated, may hold values from 0.1 to 1.9
- routing: int32 [16384, 2], P(('sp', 'tp')), may hold values from 0 to 63, as said below
- route_weight: float32 [16384, 2], P(('sp', 'tp')), may hold values from 0.3 to 1.5
- gate_weight: bfloat16 [64, 2048, 1024], P('sp', None, 'tp'), may hold values from -0.125 to 0.125
- up_weight: bfloat16 [64, 2048, 1024], P('sp', None, 'tp'), may hold values from -0.125 to 0.125
- down_weight: bfloat16 [64, 1024, 2048], P('sp', 'tp'), may hold values from -0.1875 to 0.1875
Outputs:
- result: bfloat16 [16384, 2048], P(('sp', 'tp'))
Inputs may be any that keep to these rules, and one draw needn't show every extreme that they name: `routing`: each row names 2 different experts of one group (experts g * 16 to g * 16 + 15). In each aligned block of 64 rows (the rows of one device) no expert is named by more than 4 rows; one group, the same for all blocks, has each of its experts named by exactly 4 rows of every block.
All inputs are finite; a program needn't handle non-finite values.
Results may differ from a plain program's by a relative error of at most 0.017.
Values may be sent and summed in bfloat16 or wider, within the bound.
A program may use at most 128 MiB of HBM per device.

v0:
```python
import math

import jax
import jax.numpy as jnp
from jax import lax
from jax.sharding import PartitionSpec as P

HW = 128
HN = 64
GROUPS = 4


epsilon = 1e-06


def sent_together(arrays, axis, dim, along):
    both = jnp.concatenate(arrays, axis=along)
    whole, at, outs = (lax.all_gather(both, axis, axis=dim, tiled=True), 0, [])
    for a in arrays:
        outs.append(lax.slice_in_dim(whole, at, at + a.shape[along], axis=along))
        at += a.shape[along]
    return tuple(outs)


def globalize(pieces, shard_rows):
    shards = pieces.shape[0] // shard_rows
    grid = pieces.reshape(shards, shard_rows, pieces.shape[1])
    endings = grid[:, -1, :]
    offsets = jnp.cumsum(endings, axis=0) - endings
    return (grid + offsets[:, None, :]).reshape(pieces.shape)


def head_block(
    state, queries, query_decay, keys, values, key_decay, first_key, first_query, head_width
):
    highest_old, weight_sum, weighted = state
    query_rows = queries.shape[0]
    head_count = query_decay.shape[1]
    key_rows = keys.shape[0]
    grid_query = queries.reshape(query_rows, head_count, head_width)
    grid_key = keys.reshape(key_rows, head_count, head_width)
    grid_value = values.reshape(key_rows, head_count, head_width)
    scores = jnp.einsum("thd,phd->htp", grid_query, grid_key, preferred_element_type=jnp.float32)
    scores = scores * head_width ** (-0.5) + query_decay.T[:, :, None] - key_decay.T[:, None, :]
    query_place = first_query + jnp.arange(query_rows, dtype=jnp.int32)
    key_place = first_key + jnp.arange(key_rows, dtype=jnp.int32)
    scores = jnp.where(key_place[None, None, :] <= query_place[None, :, None], scores, -jnp.inf)
    highest = jnp.maximum(highest_old, jnp.max(scores, axis=2))
    weights = jnp.exp(scores - highest[:, :, None])
    shrink = jnp.exp(highest_old - highest)
    weight_sum = weight_sum * shrink + jnp.sum(weights, axis=2)
    product = jnp.einsum(
        "htp,phd->htd", weights.astype(jnp.bfloat16), grid_value, preferred_element_type=jnp.float32
    )
    weighted = weighted * shrink[:, :, None] + product
    return (highest, weight_sum, weighted)


def fresh_state(head_count, shard_rows, head_width):
    return (
        jnp.full((head_count, shard_rows), -1e30, jnp.float32),
        jnp.zeros((head_count, shard_rows), jnp.float32),
        jnp.zeros((head_count, shard_rows, head_width), jnp.float32),
    )


def finish(state, shard_rows):
    highest, weight_sum, weighted = state
    mixed_heads = weighted / weight_sum[:, :, None]
    joined = jnp.transpose(mixed_heads, (1, 0, 2))
    return joined.reshape(shard_rows, weighted.shape[0] * weighted.shape[2]).astype(jnp.bfloat16)


def body(
    residual,
    query_wide,
    key_wide,
    value_wide,
    query_narrow,
    key_narrow,
    value_narrow,
    gate_wide,
    gate_narrow,
    out_wide,
    out_narrow,
    norm_gain,
    routing,
    route_weight,
    gate_weight,
    up_weight,
    down_weight,
):
    shard_rows = query_wide.shape[0]
    half_rows = shard_rows // 2
    sp_place = lax.axis_index("sp")
    first_query = sp_place * shard_rows
    running_wide = jnp.cumsum(jax.nn.log_sigmoid(gate_wide), axis=0)
    running_narrow = jnp.cumsum(jax.nn.log_sigmoid(gate_narrow), axis=0)
    pieces_wide, pieces_narrow = sent_together((running_wide, running_narrow), "sp", 0, 1)
    every_wide = globalize(pieces_wide, shard_rows)
    every_narrow = globalize(pieces_narrow, shard_rows)
    late_first = first_query + half_rows
    halves = []
    for place, part_wide, part_narrow in (
        (first_query, query_wide[:half_rows], query_narrow[:half_rows]),
        (late_first, query_wide[half_rows:], query_narrow[half_rows:]),
    ):
        halves.append(
            (
                place,
                part_wide,
                part_narrow,
                lax.dynamic_slice_in_dim(every_wide, place, half_rows, 0),
                lax.dynamic_slice_in_dim(every_narrow, place, half_rows, 0),
            )
        )

    def half_state():
        return (
            fresh_state(gate_wide.shape[1], half_rows, HW),
            fresh_state(gate_narrow.shape[1], half_rows, HN),
        )

    state = (half_state(), half_state())
    keys_wide, values_wide, keys_narrow, values_narrow = sent_together(
        (key_wide, value_wide, key_narrow, value_narrow), "sp", 0, 1
    )
    span_rows = keys_wide.shape[0]
    block_size = math.gcd(span_rows, 2048)

    def visit(carried, position):
        inside = position * block_size

        def take_block(source):
            return lax.dynamic_slice_in_dim(source, inside, block_size, 0)

        def take_decay(source):
            return lax.dynamic_slice_in_dim(source, inside, block_size, 0)

        block_kw = take_block(keys_wide)
        block_vw = take_block(values_wide)
        block_kn = take_block(keys_narrow)
        block_vn = take_block(values_narrow)
        block_dw = take_decay(every_wide)
        block_dn = take_decay(every_narrow)

        def one_half(current, half):
            place, part_wide, part_narrow, query_decay_wide, query_decay_narrow = half

            def work(inner):
                first = head_block(
                    inner[0],
                    part_wide,
                    query_decay_wide,
                    block_kw,
                    block_vw,
                    block_dw,
                    inside,
                    place,
                    HW,
                )
                second = head_block(
                    inner[1],
                    part_narrow,
                    query_decay_narrow,
                    block_kn,
                    block_vn,
                    block_dn,
                    inside,
                    place,
                    HN,
                )
                return (first, second)

            def skip(inner):
                return inner

            return lax.cond(inside <= place + half_rows - 1, work, skip, current)

        updated = (one_half(carried[0], halves[0]), one_half(carried[1], halves[1]))
        return (updated, None)

    state, _ = lax.scan(visit, state, jnp.arange(span_rows // block_size, dtype=jnp.int32))
    att_wide = jnp.concatenate(
        [finish(state[0][0], half_rows), finish(state[1][0], half_rows)], axis=0
    )
    att_narrow = jnp.concatenate(
        [finish(state[0][1], half_rows), finish(state[1][1], half_rows)], axis=0
    )
    own_rows = residual.shape[0]
    heads_wide, heads_narrow = (
        lax.all_to_all(att_wide, "tp", split_axis=0, concat_axis=1, tiled=True),
        lax.all_to_all(att_narrow, "tp", split_axis=0, concat_axis=1, tiled=True),
    )
    mixed = jnp.dot(heads_wide, out_wide, preferred_element_type=jnp.float32)
    mixed = mixed + jnp.dot(heads_narrow, out_narrow, preferred_element_type=jnp.float32)
    middle = (residual.astype(jnp.float32) + mixed).astype(jnp.bfloat16)
    middle_wide = middle.astype(jnp.float32)
    spread = jnp.mean(middle_wide * middle_wide, axis=1, keepdims=True)
    normed = (middle_wide * lax.rsqrt(spread + epsilon) * norm_gain).astype(jnp.bfloat16)
    features = normed.shape[1]
    chosen_count = routing.shape[1]
    expert_count = gate_weight.shape[0] * lax.axis_size("sp")
    capacity = own_rows * GROUPS // expert_count
    flat_routes = routing.reshape(-1)
    matches = (flat_routes[:, None] == jnp.arange(expert_count, dtype=jnp.int32)[None, :]).astype(
        jnp.int32
    )
    ranking = jnp.sum((jnp.cumsum(matches, axis=0) - matches) * matches, axis=1)
    placing = flat_routes * capacity + ranking
    picker = (
        placing[None, :] == jnp.arange(expert_count * capacity, dtype=jnp.int32)[:, None]
    ).astype(jnp.bfloat16)
    picker = jnp.sum(picker.reshape(expert_count * capacity, own_rows, chosen_count), axis=2)
    outgoing = jnp.dot(picker, normed, preferred_element_type=jnp.float32).astype(jnp.bfloat16)
    outgoing = outgoing.reshape(expert_count, capacity, features)
    arrived = lax.all_to_all(outgoing, "sp", split_axis=0, concat_axis=0, tiled=True)
    pooled = lax.all_gather(arrived.reshape(-1, features), "tp", axis=0, tiled=True)
    gate_value = jnp.dot(pooled, gate_weight[0], preferred_element_type=jnp.float32)
    up_value = jnp.dot(pooled, up_weight[0], preferred_element_type=jnp.float32)
    hidden = (jax.nn.silu(gate_value) * up_value).astype(jnp.bfloat16)
    answers = lax.psum_scatter(
        jnp.dot(hidden, down_weight[0], preferred_element_type=jnp.float32).astype(jnp.bfloat16),
        "tp",
        scatter_dimension=0,
        tiled=True,
    )
    returned = lax.all_to_all(
        answers.reshape(expert_count, capacity, features),
        "sp",
        split_axis=0,
        concat_axis=0,
        tiled=True,
    )
    picked = jnp.take(returned.reshape(expert_count * capacity, features), placing, axis=0)
    picked = picked.reshape(own_rows, chosen_count, features).astype(jnp.float32)
    combined = jnp.sum(route_weight[:, :, None] * picked, axis=1)
    return (middle_wide + combined).astype(jnp.bfloat16)


def solution(mesh):
    placed = (
        P(("sp", "tp"), None),
        P("sp", "tp"),
        P("sp", "tp"),
        P("sp", "tp"),
        P("sp", "tp"),
        P("sp", "tp"),
        P("sp", "tp"),
        P("sp", "tp"),
        P("sp", "tp"),
        P(),
        P(),
        P(),
        P(("sp", "tp"), None),
        P(("sp", "tp"), None),
        P("sp", None, "tp"),
        P("sp", None, "tp"),
        P("sp", "tp", None),
    )
    return jax.shard_map(
        body, mesh=mesh, in_specs=placed, out_specs=P(("sp", "tp"), None), check_vma=False
    )
```

profile of v0, /device:TPU:1, one launch (start us, length us, event | category | flops | bytes accessed | tf_op | source)
XLA Modules:
  0.0 530.6 jit_solution(731115562800236567)
XLA Ops:
  18.2 48.7 %all_gather.10 = f32[16384,3]{0,1:T(4,128)S(1)} all-gather(f32[256,3]{0,1:T(4,128)S(1)} %pad_maximum_fusion.3), channel_id=1, replica_groups=mesh['sp'=64,'tp'=4] {'sp'}, dimensions={0}, use_global_device_ids=true | all-gather | bytes 199680 | tf_op jit(solution)/shard_map/all_gather | solution.py:18
  67.1 4.9 copy.106
  72.0 1.2 reduce-window_subtract_fusion
  73.7 9.2 %reshape.388 = f32[64,256,1]{2,1,0:T(8,128)} reshape(f32[16384]{0:T(1024)S(1)} %slice_reduce_fusion) | data formatting | bytes 131072 | tf_op jit(solution)/shard_map/reshape | solution.py:27
  82.9 1.7 fusion.75
  85.5 1.2 constant_dynamic-slice_fusion.7
  89.4 32.0 %all-gather.3.cloned.1.call-done = bf16[16384,512]{0,1:T(8,128)(2,1)} async-done(((bf16[256,512]{0,1:T(8,128)(2,1)}), bf16[16384,512]{0,1:T(8,128)(2,1)}) %all-gather.3.cloned.1.call-update) | async-done | bytes 16777232 | tf_op jit(solution)/shard_map/all_gather | solution.py:18
  121.4 12.1 %fusion.72 = (bf16[16384,128]{0,1:T(8,128)(2,1)}, bf16[16384,128]{0,1:T(8,128)(2,1)}, bf16[16384,128]{0,1:T(8,128)(2,1)}, bf16[16384,128]{0,1:T(8,128)(2,1)}) fusion(bf16[16384,512]{0,1:T(8,128)(2,1)} %all-gather.3.cloned.1.call-done), kind=kLoop, calls=%fused_computation.146 | loop fusion | bytes 33554432 | tf_op jit(solution)/shard_map/slice | solution.py:20
  138.6 89.0 %while.35 = (s32[]{:T(128)}, f32[1,128]{1,0:T(1,128)}, f32[1,128]{1,0:T(1,128)}, f32[1,128,128]{2,1,0:T(8,128)S(1)}, f32[2,128]{1,0:T(2,128)}, /*index=5*/f32[2,...) while((s32[]{:T(128)}, f32[1,128]{1,0:T(1,128)}, ...), condition=%wide.region_19.20_spmd, body=%wide.region_6.19_spmd.sunk | while | flops 552212480 | bytes 35769752 | solution.py:183
  138.6 1.2 dynamic_slice.78
  140.5 1.3 constant_dynamic-slice_fusion.15
  141.8 2.1 constant_dynamic-slice_fusion.16
  143.8 2.1 constant_dynamic-slice_fusion.14
  146.9 1.3 copy.144
  148.2 5.7 %conditional.4 = ((f32[1,128]{1,0:T(1,128)}, f32[1,128]{1,0:T(1,128)}, f32[1,128,128]{2,1,0:T(8,128)S(1)}, f32[2,128]{1,0:T(2,128)}, f32[2,128]{1,0:T(2,128)}, /*index=5*/f32[2,128,64]{1,2,0:T(8,128)S(1)})) conditional(s32[]{:T(128)} %convert_element_type.151, (f32[1,128]{1,0:T(1,128)}, f32[1,128]{1,0:T(1,128)}, f32[1,128,128]{2,1,0:T(8,128)S(1)}, ...), branch_computations={%region_7.7_spmd, %region_8.12_spmd} | conditional | flops 276106240 | bytes 14714172 | solution.py:178
  148.6 1.5 fusion.68
  153.9 5.6 %conditional.5 = ((f32[1,128]{1,0:T(1,128)}, f32[1,128]{1,0:T(1,128)}, f32[1,128,128]{2,1,0:T(8,128)S(1)}, f32[2,128]{1,0:T(2,128)}, f32[2,128]{1,0:T(2,128)}, /*index=5*/f32[2,128,64]{1,2,0:T(8,128)S(1)})) conditional(s32[]{:T(128)} %convert_element_type.152, (f32[1,128]{1,0:T(1,128)}, f32[1,128]{1,0:T(1,128)}, f32[1,128,128]{2,1,0:T(8,128)S(1)}, ...), branch_computations={%region_13.13_spmd, %region_14.18_spmd} | conditional | flops 276106240 | bytes 14714172 | solution.py:178
  154.2 1.5 fusion.70
  161.4 1.3 constant_dynamic-slice_fusion.15
  162.7 2.1 constant_dynamic-slice_fusion.16
  164.7 2.1 constant_dynamic-slice_fusion.14
  167.8 1.3 copy.144
  171.1 1.3 constant_dynamic-slice_fusion.15
  172.4 2.1 constant_dynamic-slice_fusion.16
  174.5 2.1 constant_dynamic-slice_fusion.14
  177.6 1.3 copy.144
  180.8 1.3 constant_dynamic-slice_fusion.15
  182.1 2.1 constant_dynamic-slice_fusion.16
  184.2 2.1 constant_dynamic-slice_fusion.14
  187.3 1.3 copy.144
  190.6 1.3 constant_dynamic-slice_fusion.15
  191.9 2.1 constant_dynamic-slice_fusion.16
  193.9 2.1 constant_dynamic-slice_fusion.14
  197.0 1.3 copy.144
  200.3 1.3 constant_dynamic-slice_fusion.15
  201.6 2.1 constant_dynamic-slice_fusion.16
  203.7 2.1 constant_dynamic-slice_fusion.14
  206.8 1.3 copy.144
  210.0 1.3 constant_dynamic-slice_fusion.15
  211.3 2.1 constant_dynamic-slice_fusion.16
  213.4 2.1 constant_dynamic-slice_fusion.14
  216.5 1.3 copy.144
  219.7 1.3 constant_dynamic-slice_fusion.15
  221.0 2.1 constant_dynamic-slice_fusion.16
  223.1 2.1 constant_dynamic-slice_fusion.14
  226.2 1.3 copy.144
  229.1 4.1 all-to-all-start
  234.6 3.0 all-to-all-done
  237.6 3.3 all-to-all-start.1
  241.2 2.1 fusion.53
  243.2 2.1 all-to-all-done.1
  247.3 1.2 reshape.376
  248.5 115.7 %all_to_all.48 = bf16[64,4,2048]{2,1,0:T(4,128)(2,1)S(1)} all-to-all(bf16[64,4,2048]{2,1,0:T(4,128)(2,1)} %reshape.376), channel_id=1, replica_groups=mesh['sp'=64,'tp'=4] {'sp'}, dimensions={0} | all-to-all | bytes 2097152 | tf_op jit(solution)/shard_map/all_to_all | solution.py:217
  365.3 45.8 %all-gather.5.cloned.1.call-done = bf16[1024,2048]{1,0:T(8,128)(2,1)} async-done(((bf16[256,2048]{1,0:T(8,128)(2,1)}), bf16[1024,2048]{1,0:T(8,128)(2,1)}) %all-gather.5.cloned.1.call-update) | async-done | bytes 4194320 | tf_op jit(solution)/shard_map/all_gather | solution.py:218
  411.1 4.8 fusion.39
  415.9 9.1 %convolution_convert_fusion = bf16[1024,2048]{1,0:T(8,128)(2,1)} fusion(bf16[1024,2048]{1,0:T(8,128)(2,1)} %all-gather.5.cloned.1.call-done, bf16[1,256,2048]{2,1,0:T(8,128)(2,1)S(1)} %copy-done.31, bf16[1,2048,256]{2,1,0:T(8,128)(2,1)} %param.38, f32[1024,256]{1,0:T(8,128)} %fusion.39), kind=kOutput, calls=%fused_computation.63 | convolution fusion | flops 2151153664 | bytes 11534336 | tf_op jit(solution)/shard_map/dot_general | solution.py:223
  425.0 50.0 %reduce-scatter.2.cloned.1.call-done = bf16[256,2048]{1,0:T(8,128)(2,1)} async-done(((bf16[1024,2048]{1,0:T(8,128)(2,1)}), bf16[256,2048]{1,0:T(8,128)(2,1)}) %reduce-scatter.2.cloned.1.call-update) | async-done | bytes 1048592 | tf_op jit(solution)/shard_map/reduce_scatter | solution.py:222
  475.0 2.2 reshape.378
  477.2 10.9 %all-to-all-start.3 = ((bf16[64,4,2048]{2,1,0:T(4,128)(2,1)}), bf16[64,4,2048]{2,1,0:T(4,128)(2,1)}, u32[]{:S(2)}, u32[]{:S(2)}) async-start(bf16[64,4,2048]{2,1,0:T(4,128)(2,1)} %reshape.378), calls=%async_computation.4 | async-start | bytes 2097152 | tf_op jit(solution)/shard_map/all_to_all | solution.py:228
  488.7 27.6 %all-to-all-done.3 = bf16[64,4,2048]{2,1,0:T(4,128)(2,1)} async-done(((bf16[64,4,2048]{2,1,0:T(4,128)(2,1)}), bf16[64,4,2048]{2,1,0:T(4,128)(2,1)}, u32[]{:S(2)}, u32[]{:S(2)}) %all-to-all-start.3) | async-done | bytes 1048608 | tf_op jit(solution)/shard_map/all_to_all | solution.py:228
  516.2 1.3 reshape.379
  517.6 1.7 gather_fusion
  519.3 1.4 gather.7
  520.7 2.5 multiply_reduce_fusion
  (208 shorter events, 52.5 us)
Async XLA Ops:
  6.5 238.8 %copy-start = (bf16[512,2048]{1,0:T(8,128)(2,1)S(1)}, bf16[512,2048]{1,0:T(8,128)(2,1)}, u32[]{:S(2)}) copy-start(bf16[512,2048]{1,0:T(8,128)(2,1)} %param.33) | copy-start | bytes 6291460
  6.5 114.8 %all-gather.3.cloned.1.call-start = ((), (), s32[]{:S(2)}) async-start(), calls=%async_computation.5 | async-start | bytes 17039360 | tf_op jit(solution)/shard_map/all_gather | solution.py:18
  14.3 3.9 copy-start.25
  73.7 13.8 %copy-start.22 = (s32[64,2]{0,1:T(2,128)S(1)}, s32[64,2]{0,1:T(2,128)}, u32[]{:S(2)}) copy-start(s32[64,2]{0,1:T(2,128)} %param.35) | copy-start | bytes 1540
  73.7 15.0 %copy-start.9 = (bf16[256,128]{1,0:T(8,128)(2,1)S(1)}, bf16[256,128]{1,0:T(8,128)(2,1)}, u32[]{:S(2)}) copy-start(bf16[256,128]{1,0:T(8,128)(2,1)} %param.24) | copy-start | bytes 196612
  148.3 1.9 copy-start.11
  148.5 2.3 copy-start.20
  148.5 2.9 copy-start.1
  148.5 2.9 copy-start.17
  148.5 2.9 copy-start.30
  150.8 1.5 copy-start.8
  150.8 1.4 copy-start.21
  151.4 1.3 copy-start.14
  152.8 1.2 copy-start.15
  153.9 1.8 copy-start.10
  154.2 2.3 copy-start.18
  154.2 2.8 copy-start.2
  154.2 2.8 copy-start.16
  154.2 2.8 copy-start.29
  156.5 1.4 copy-start.7
  156.5 1.3 copy-start.19
  157.0 1.3 copy-start.12
  158.3 1.2 copy-start.13
  227.6 17.8 %copy-start.5 = (bf16[64,2048]{1,0:T(8,128)(2,1)S(1)}, bf16[64,2048]{1,0:T(8,128)(2,1)}, u32[]{:S(2)}) copy-start(bf16[64,2048]{1,0:T(8,128)(2,1)} %param.23) | copy-start | bytes 786436
  229.1 8.6 %all-to-all-start = ((bf16[4,64,128]{2,1,0:T(8,128)(2,1)}), bf16[4,64,128]{2,1,0:T(8,128)(2,1)S(1)}, u32[]{:S(2)}, u32[]{:S(2)}) async-start(bf16[4,64,128]{2,1,0:T(8,128)(2,1)} %bitcast.37), calls=%async_computation | async-start | bytes 131072 | tf_op jit(solution)/shard_map/all_to_all | solution.py:192
  237.6 7.7 %all-to-all-start.1 = ((bf16[4,64,128]{2,1,0:T(8,128)(2,1)}), bf16[4,64,128]{2,1,0:T(8,128)(2,1)S(1)}, u32[]{:S(2)}, u32[]{:S(2)}) async-start(bf16[4,64,128]{2,1,0:T(8,128)(2,1)} %bitcast.43), calls=%async_computation.1 | async-start | bytes 131072 | tf_op jit(solution)/shard_map/all_to_all | solution.py:193
  240.9 170.2 %all-gather.5.cloned.1.call-start = ((), (), s32[]{:S(2)}) async-start(), calls=%async_computation.6 | async-start | bytes 5242880 | tf_op jit(solution)/shard_map/all_gather | solution.py:218
  243.2 3.6 copy-start.6
  243.2 3.6 copy-start.24
  246.0 0.8 copy-start.3
  365.3 50.6 %copy-start.31 = (bf16[1,256,2048]{2,1,0:T(8,128)(2,1)S(1)}, bf16[1,256,2048]{2,1,0:T(8,128)(2,1)}, u32[]{:S(2)}) copy-start(bf16[1,256,2048]{2,1,0:T(8,128)(2,1)} %param.39) | copy-start | bytes 3145732
  365.3 109.7 %reduce-scatter.2.cloned.1.call-start = ((), (), s32[]{:S(2)}) async-start(), calls=%async_computation.7 | async-start | bytes 5242880 | tf_op jit(solution)/shard_map/reduce_scatter | solution.py:222
  425.0 63.2 %copy-start.23 = (s32[64,2]{0,1:T(2,128)S(1)}, s32[64,2]{0,1:T(2,128)}, u32[]{:S(2)}) copy-start(s32[64,2]{0,1:T(2,128)} %param.35) | copy-start | bytes 1540
  425.0 63.4 %copy-start.28 = (f32[64,2]{0,1:T(2,128)S(1)}, f32[64,2]{0,1:T(2,128)}, u32[]{:S(2)}) copy-start(f32[64,2]{0,1:T(2,128)} %param.36) | copy-start | bytes 1540
  425.0 63.5 %copy-start.27 = (pred[64,2]{0,1:T(4,128)(4,1)S(1)}, pred[64,2]{0,1:T(4,128)(4,1)}, u32[]{:S(2)}) copy-start(pred[64,2]{0,1:T(4,128)(4,1)} %get-tuple-element.875) | copy-start | bytes 388
  425.0 63.6 %copy-start.26 = (s32[128]{0:T(128)S(1)}, s32[128]{0:T(128)}, u32[]{:S(2)}) copy-start(s32[128]{0:T(128)} %copy-done.25) | copy-start | bytes 1540
  477.2 39.0 %all-to-all-start.3 = ((bf16[64,4,2048]{2,1,0:T(4,128)(2,1)}), bf16[64,4,2048]{2,1,0:T(4,128)(2,1)}, u32[]{:S(2)}, u32[]{:S(2)}) async-start(bf16[64,4,2048]{2,1,0:T(4,128)(2,1)} %reshape.378), calls=%async_computation.4 | async-start | bytes 2097152 | tf_op jit(solution)/shard_map/all_to_all | solution.py:228
  519.3 4.0 copy-start.4
Sparse Core Ops, SparseCore 0:
  11.3 110.0 all-gather.2
  365.4 45.6 all-gather.4
  425.1 49.8 reduce-scatter.1
where the time goes:
time: 533 us; the launch traced here: 531 us
  blocking collectives  164 us (31%)
  waiting for transfers between devices  161 us (30%)
  local copies, waits for them, and re-layouts  127 us (24%)
  matrix products  23.7 us (4%)
  starting transfers between devices  18.5 us (3%)
  other arithmetic  16.4 us (3%)
  between operations  13.5 us (3%)
  loops' own time  6.28 us (1%)
    all_to_all x1, blocking collectives, body(): lax.all_to_all(outgoing, 'sp', split_axis=0, concat_axis=0, tiled=True)  116 us
    dynamic_slice x32, local copies, waits for them, and re-layouts, take_block(): return lax.dynamic_slice_in_dim(source, inside, block_size, 0)  51.8 us
    reduce_scatter x1, waiting for transfers between devices, body(): lax.psum_scatter(jnp.dot(hidden, down_weight[0], preferred_element_type=j...  50 us
    all_gather x1, blocking collectives, sent_together(): whole, at, outs = (lax.all_gather(both, axis, axis=dim, tiled=True), 0, [])  48.7 us
    all_gather x1, waiting for transfers between devices, body(): lax.all_gather(arrived.reshape(-1, features), 'tp', axis=0, tiled=True)  45.8 us
    all_gather x1, waiting for transfers between devices, sent_together(): whole, at, outs = (lax.all_gather(both, axis, axis=dim, tiled=True), 0, [])  32 us
    all_to_all x1, waiting for transfers between devices, body(): lax.all_to_all(answers.reshape(expert_count, capacity, features), 'sp', s...  27.6 us
    slice x4, local copies, waits for them, and re-layouts, sent_together(): outs.append(lax.slice_in_dim(whole, at, at + a.shape[along], axis=along))  17.3 us
  transfers between devices with their start and end apart: 6, of which 6 were waited for; matrix products, arithmetic and copies ran while one was open for 6% of the time, Pallas kernels for 0%

commit v1 on v0

v1 whole, which is shorter than its diff:
```python
import functools
import math

import jax
import jax.numpy as jnp
from jax import lax
from jax.experimental import pallas as pl
from jax.experimental.pallas import tpu as pltpu
from jax.sharding import PartitionSpec as P

MESH = pl.DeviceIdType.MESH
F32, BF16 = jnp.float32, jnp.bfloat16
HW = 128
HN = 64
GROUPS = 4
LOG2E = math.log2(math.e)
NEG = -1e30
epsilon = 1e-06


def attention_kernel(
    dims, q_ref, kd_ref, v_ref, tot_ref, att_ref,
    qb, kb, vb, tt, drow, mb, acc, ob, sb, orv, srv, ab, ar,
    q_s, q_r, up_s, up_r, dn_s, dn_r, pr_s, pr_r, t1_s, t1_r, t2_s, t2_r, o_s, o_r, y_s, y_r, loc,
):
    nz, nx, ny = dims
    half = nz // 2
    sp, y = lax.axis_index("sp"), lax.axis_index("tp")
    c = lax.rem(sp, 2)
    x = lax.rem(sp // 2, nx)
    z = sp // (2 * nx)
    xc = x * 2 + c

    def at(z_, x_, c_, y_):
        return ((z_ * nx + x_) * 2 + c_, y_)

    def zup(i):
        return lax.rem(z + i, nz)

    def zdn(i):
        return lax.rem(z - i + nz, nz)

    def in_plane(i):
        other = lax.rem(xc + i, 2 * nx)
        return at(z, other // 2, lax.rem(other, 2), y)

    def remote(src, dst, send, recv, device):
        return pltpu.make_async_remote_copy(
            src_ref=src, dst_ref=dst, send_sem=send, recv_sem=recv, device_id=device, device_id_type=MESH
        )

    barrier = pltpu.get_barrier_semaphore()

    def greet(device):
        pl.semaphore_signal(barrier, inc=1, device_id=device, device_id_type=MESH)

    for i in range(1, nz):
        greet(at(zup(i), x, c, y))
    for i in range(1, 2 * nx):
        greet(in_plane(i))
    for i in range(1, ny):
        greet(at(z, x, c, lax.rem(y + i, ny)))
    pl.semaphore_wait(barrier, nz - 1 + 2 * nx - 1 + ny - 1)

    up_dev, dn_dev, pr_dev = at(zup(1), x, c, y), at(zdn(1), x, c, y), at(z, x, 1 - c, y)

    def up_copy(s, j):
        zb = zdn(s)
        src = (kb, vb)[j].at[zb, c]
        return remote(src, src, up_s.at[s, j], up_r.at[s, j], up_dev)

    def dn_copy(s, j):
        zb = zup(s)
        src = (kb, vb)[j].at[zb, c]
        return remote(src, src, dn_s.at[s, j], dn_r.at[s, j], dn_dev)

    def pr_copy(zb, j):
        src = (kb, vb)[j].at[zb, c]
        return remote(src, src, pr_s.at[zb, j], pr_r.at[zb, j], pr_dev)

    def pr_wait(zb, j):
        dst = (kb, vb)[j].at[zb, 1 - c]
        remote(dst, dst, pr_s.at[zb, j], pr_r.at[zb, j], pr_dev).wait_recv()

    def own_up(j):
        return remote((kd_ref, v_ref)[j], (kb, vb)[j].at[z, c], up_s.at[0, j], up_r.at[0, j], up_dev)

    def own_dn(j):
        return remote((kd_ref, v_ref)[j], (kb, vb)[j].at[z, c], dn_s.at[0, j], dn_r.at[0, j], dn_dev)

    def own_pr(j):
        return remote((kd_ref, v_ref)[j], (kb, vb)[j].at[z, c], pr_s.at[z, j], pr_r.at[z, j], pr_dev)

    def up_has(s, j):
        return s < half or (s == half and j == 0)

    def dn_has(s, j):
        return s < half or (s == half and j == 1)

    for j in range(2):
        if up_has(1, j):
            own_up(j).start()
        if dn_has(1, j):
            own_dn(j).start()

    def t1_copy(i):
        return remote(tot_ref, tt.at[z, xc], t1_s.at[i - 1], t1_r.at[i - 1], in_plane(i))

    def t2_copy(i):
        return remote(tt.at[z], tt.at[z], t2_s.at[i - 1], t2_r.at[i - 1], at(zup(i), x, c, y))

    def q_copy(i):
        return remote(q_ref, qb.at[x], q_s.at[i - 1], q_r.at[i - 1], at(z, lax.rem(x + i, nx), c, y))

    for i in range(1, 2 * nx):
        t1_copy(i).start()
    for i in range(1, nx):
        q_copy(i).start()
    for j in range(2):
        own_pr(j).start()
    local = [
        pltpu.make_async_copy(tot_ref, tt.at[z, xc], loc.at[0]),
        pltpu.make_async_copy(q_ref, qb.at[x], loc.at[1]),
        pltpu.make_async_copy(kd_ref, kb.at[z, c], loc.at[2]),
        pltpu.make_async_copy(v_ref, vb.at[z, c], loc.at[3]),
    ]
    for copy in local:
        copy.start()
    mb[...] = jnp.full(mb.shape, NEG, F32)
    acc[...] = jnp.zeros(acc.shape, F32)
    local[0].wait()
    for i in range(1, 2 * nx):
        other = lax.rem(xc - i + 2 * nx, 2 * nx)
        remote(tot_ref, tt.at[z, other], t1_s.at[i - 1], t1_r.at[i - 1], in_plane(i)).wait_recv()
    for i in range(1, nz):
        t2_copy(i).start()
    for copy in local[1:]:
        copy.wait()

    def relay(s):
        for j in range(2):
            if up_has(s, j):
                slot = (kb, vb)[j].at[zdn(s), c]
                remote(slot, slot, up_s.at[s - 1, j], up_r.at[s - 1, j], up_dev).wait_recv()
                if up_has(s + 1, j):
                    up_copy(s, j).start()
                pr_copy(zdn(s), j).start()
            if dn_has(s, j):
                slot = (kb, vb)[j].at[zup(s), c]
                remote(slot, slot, dn_s.at[s - 1, j], dn_r.at[s - 1, j], dn_dev).wait_recv()
                if dn_has(s + 1, j):
                    dn_copy(s, j).start()
                pr_copy(zup(s), j).start()

    lane = lax.broadcasted_iota(jnp.int32, (1, 128), 1)
    low = lane < HN

    def head_offsets(zb):
        def plane(p, run):
            whole = jnp.zeros((1, 128), F32)
            for k in range(2 * nx):
                whole = whole + tt[p, k]
            return run + jnp.where(p < zb, whole, 0.0)
        run = lax.fori_loop(0, nz, plane, jnp.zeros((1, 128), F32))
        for k in range(2 * nx):
            run = run + jnp.where(k < 2 * x, tt[zb, k], 0.0)
        return run, run + tt[zb, 2 * x]

    def make_drow(zb):
        offs = head_offsets(zb)
        parts = [kb[zb, k, pl.ds(256, 16), :].astype(F32) for k in range(2)]
        for h in range(3):
            pieces = []
            for k in range(2):
                off = jnp.sum(jnp.where(lane == h, offs[k], 0.0), axis=1, keepdims=True)
                p = parts[k]
                pieces.append(p[3 * h:3 * h + 1] + p[3 * h + 1:3 * h + 2] + p[3 * h + 2:3 * h + 3] + off)
            drow[h] = jnp.concatenate(pieces, axis=1)

    scales = (HW ** -0.5 * LOG2E, HN ** -0.5 * LOG2E, HN ** -0.5 * LOG2E)

    def tile(zb, xq, masked):
        q = qb[xq]
        qw, qn = q[:, :128], q[:, 128:]
        zero = jnp.zeros_like(qn)
        heads = (qw, jnp.where(low, qn, zero), jnp.where(low, zero, qn))
        keys = jnp.concatenate([kb[zb, 0, :256, :], kb[zb, 1, :256, :]], axis=0)
        vals = jnp.concatenate([vb[zb, 0], vb[zb, 1]], axis=0)
        ones = jnp.ones((512, 128), BF16)
        if masked:
            rows = lax.broadcasted_iota(jnp.int32, (256, 512), 0) + (xq * 512 + c * 256)
            cols = lax.broadcasted_iota(jnp.int32, (256, 512), 1) + x * 512
            seen = cols <= rows
        for h in range(3):
            side = slice(0, 128) if h == 0 else slice(128, 256)
            s = lax.dot_general(heads[h], keys[:, side], (((1,), (1,)), ((), ())), preferred_element_type=F32)
            r = s * scales[h] - drow[h]
            if masked:
                r = jnp.where(seen, r, NEG)
            old = mb[xq, h]
            new = jnp.maximum(old, jnp.max(r, axis=1, keepdims=True))
            p = jnp.exp2(r - jnp.concatenate([new] * 4, axis=1)).astype(BF16)
            shrink = jnp.exp2(old - new)
            mb[xq, h] = new
            right = jnp.concatenate([vals[:, side], ones], axis=1)
            pv = jnp.dot(p, right, preferred_element_type=F32)
            acc[xq, h] = acc[xq, h] * jnp.concatenate([shrink, shrink], axis=1) + pv

    def both(zb):
        make_drow(zb)

        def one(xq, carry):
            tile(zb, xq, False)
            return carry
        lax.fori_loop(0, nx, one, 0)

    relay(1)
    for i in range(1, nx):
        src = lax.rem(x - i + nx, nx)
        remote(q_ref, qb.at[src], q_s.at[i - 1], q_r.at[i - 1], at(z, src, c, y)).wait_recv()
    for i in range(1, nz):
        slot = tt.at[zdn(i)]
        remote(slot, slot, t2_s.at[i - 1], t2_r.at[i - 1], at(zdn(i), x, c, y)).wait_recv()
    for j in range(2):
        pr_wait(z, j)
    make_drow(z)

    def own(xq, carry):
        @pl.when(xq >= x)
        def _():
            tile(z, xq, True)
        return carry
    lax.fori_loop(0, nx, own, 0)

    for s in range(1, half):
        relay(s + 1)
        for j in range(2):
            pr_wait(zdn(s), j)
            pr_wait(zup(s), j)
        for zb, needed in ((zdn(s), z >= s), (zup(s), z + s >= nz)):
            @pl.when(needed)
            def _():
                both(zb)
    if half == 1:
        pass
    for j in range(2):
        pr_wait(zdn(half), j)

    @pl.when(z >= half)
    def _():
        make_drow(zdn(half))

    def o_copies(i):
        dev = at(z, lax.rem(x + i, nx), c, y)
        return (
            remote(ob.at[i], orv.at[i], o_s.at[i, 0], o_r.at[i, 0], dev),
            remote(sb.at[i], srv.at[i], o_s.at[i, 1], o_r.at[i, 1], dev),
        )

    def last(k, carry):
        i = lax.rem(k + 1, nx)
        xq = lax.rem(x + i, nx)

        @pl.when(z >= half)
        def _():
            tile(zdn(half), xq, False)

        outs, lses = [], []
        for h in range(3):
            total = acc[xq, h, :, 128:]
            some = total > 0.0
            safe = jnp.where(some, total, 1.0)
            outs.append(acc[xq, h, :, :128] / safe)
            lses.append(jnp.where(some, mb[xq, h] + jnp.log2(safe), NEG))
        wide, narrow = outs[0], jnp.where(low, outs[1], outs[2])
        ob[i] = jnp.concatenate([wide, narrow], axis=1).astype(BF16)
        packed = jnp.where(lane == 0, lses[0], jnp.where(lane == 1, lses[1], lses[2]))
        sb[i] = jnp.transpose(packed)[:8]

        @pl.when(i > 0)
        def _():
            for copy in o_copies(i):
                copy.start()
        return carry
    lax.fori_loop(0, nx, last, 0)

    for i in range(1, nx):
        src = lax.rem(x - i + nx, nx)
        for copy in o_copies(i):
            copy.wait_recv()
    stats = [sb[0]] + [srv[i] for i in range(1, nx)]
    outs = [ob[0]] + [orv[i] for i in range(1, nx)]
    top = functools.reduce(jnp.maximum, stats)
    shares = [jnp.exp2(t - top) for t in stats]
    whole = functools.reduce(jnp.add, shares)
    shares = [t / whole for t in shares]
    columns = jnp.transpose(jnp.concatenate(shares + [jnp.zeros((128 - 8 * nx, 256), F32)], axis=0))
    wide = jnp.zeros((256, 128), F32)
    narrow = jnp.zeros((256, 128), F32)
    for i in range(nx):
        o = outs[i].astype(F32)
        wide = wide + columns[:, 8 * i:8 * i + 1] * o[:, :128]
        narrow = narrow + jnp.where(low, columns[:, 8 * i + 1:8 * i + 2], columns[:, 8 * i + 2:8 * i + 3]) * o[:, 128:]
    ab[...] = jnp.concatenate([wide, narrow], axis=1).astype(BF16)

    share = 256 // ny

    def rows_of(y_):
        return ab.at[pl.ds(pl.multiple_of(y_ * share, share), share), :]

    def y_copy(i):
        other = lax.rem(y + i, ny)
        return remote(rows_of(other), ar.at[y], y_s.at[i - 1], y_r.at[i - 1], at(z, x, c, other))

    for i in range(1, ny):
        y_copy(i).start()
    att_ref[y] = ab[pl.ds(pl.multiple_of(y * share, share), share), :]
    for i in range(1, ny):
        src = lax.rem(y - i + ny, ny)
        remote(rows_of(src), ar.at[src], y_s.at[i - 1], y_r.at[i - 1], at(z, x, c, src)).wait_recv()
        att_ref[src] = ar[src]

    for j in range(2):
        if up_has(1, j):
            own_up(j).wait_send()
        if dn_has(1, j):
            own_dn(j).wait_send()
        own_pr(j).wait_send()
        for s in range(1, half + 1):
            if up_has(s, j):
                if up_has(s + 1, j):
                    up_copy(s, j).wait_send()
                pr_copy(zdn(s), j).wait_send()
            if dn_has(s, j):
                if dn_has(s + 1, j):
                    dn_copy(s, j).wait_send()
                pr_copy(zup(s), j).wait_send()
    for i in range(1, 2 * nx):
        t1_copy(i).wait_send()
    for i in range(1, nz):
        t2_copy(i).wait_send()
    for i in range(1, nx):
        q_copy(i).wait_send()
        for copy in o_copies(i):
            copy.wait_send()
    for i in range(1, ny):
        y_copy(i).wait_send()


def attend(dims, q, kd, v, tot):
    nz, nx, ny = dims
    half = nz // 2
    dma = pltpu.SemaphoreType.DMA
    vmem = pl.BlockSpec(memory_space=pltpu.VMEM)
    return pl.pallas_call(
        functools.partial(attention_kernel, dims),
        out_shape=jax.ShapeDtypeStruct((ny, 256 // ny, 256), BF16),
        in_specs=[vmem] * 4,
        out_specs=vmem,
        scratch_shapes=[
            pltpu.VMEM((nx, 256, 256), BF16),
            pltpu.VMEM((nz, 2, 272, 256), BF16),
            pltpu.VMEM((nz, 2, 256, 256), BF16),
            pltpu.VMEM((nz, 2 * nx, 1, 128), F32),
            pltpu.VMEM((3, 1, 512), F32),
            pltpu.VMEM((nx, 3, 256, 128), F32),
            pltpu.VMEM((nx, 3, 256, 256), F32),
            pltpu.VMEM((nx, 256, 256), BF16),
            pltpu.VMEM((nx, 8, 256), F32),
            pltpu.VMEM((nx, 256, 256), BF16),
            pltpu.VMEM((nx, 8, 256), F32),
            pltpu.VMEM((256, 256), BF16),
            pltpu.VMEM((ny, 256 // ny, 256), BF16),
            dma((nx,)), dma((nx,)),
            dma((half + 1, 2)), dma((half + 1, 2)), dma((half + 1, 2)), dma((half + 1, 2)),
            dma((nz, 2)), dma((nz, 2)),
            dma((2 * nx,)), dma((2 * nx,)), dma((nz,)), dma((nz,)),
            dma((nx, 2)), dma((nx, 2)), dma((ny,)), dma((ny,)), dma((4,)),
        ],
        compiler_params=pltpu.CompilerParams(collective_id=1, has_side_effects=True, vmem_limit_bytes=40 * 2**20),
        cost_estimate=pl.CostEstimate(flops=10**10, bytes_accessed=10**7, transcendentals=12 * 10**6),
        name="attend",
    )(q, kd, v, tot)


def prepare(query_wide, key_wide, value_wide, query_narrow, key_narrow, value_narrow, gate_wide, gate_narrow):
    gates = jnp.concatenate([gate_wide, gate_narrow], axis=1)
    run = jnp.cumsum(jax.nn.log_sigmoid(gates).T, axis=1) * LOG2E
    tot = jnp.pad(run[:, -1], (0, 125))[None, :]
    high = lax.reduce_precision(run, 8, 7)
    mid = lax.reduce_precision(run - high, 8, 7)
    parts = jnp.stack([high, mid, run - high - mid], axis=1).reshape(9, 256)
    parts = jnp.pad(parts, ((0, 7), (0, 0))).astype(BF16)
    q = jnp.concatenate([query_wide, query_narrow], axis=1)
    kd = jnp.concatenate([jnp.concatenate([key_wide, key_narrow], axis=1), parts], axis=0)
    v = jnp.concatenate([value_wide, value_narrow], axis=1)
    return q, kd, v, tot


def body(
    residual,
    query_wide,
    key_wide,
    value_wide,
    query_narrow,
    key_narrow,
    value_narrow,
    gate_wide,
    gate_narrow,
    out_wide,
    out_narrow,
    norm_gain,
    routing,
    route_weight,
    gate_weight,
    up_weight,
    down_weight,
):
    ny = lax.axis_size("tp")
    nx = 4
    dims = (lax.axis_size("sp") // (2 * nx), nx, ny)
    own_rows = residual.shape[0]
    full_gate = lax.all_gather(gate_weight[0], "tp", axis=0)
    full_up = lax.all_gather(up_weight[0], "tp", axis=0)
    full_down = lax.all_gather(down_weight[0], "tp", axis=0, tiled=True)
    att = attend(
        dims,
        *prepare(
            query_wide, key_wide, value_wide, query_narrow, key_narrow, value_narrow, gate_wide, gate_narrow
        ),
    )
    heads_wide = jnp.transpose(att[:, :, :128], (1, 0, 2)).reshape(own_rows, 128 * ny)
    heads_narrow = jnp.transpose(att[:, :, 128:], (1, 0, 2)).reshape(own_rows, 128 * ny)
    mixed = jnp.dot(heads_wide, out_wide, preferred_element_type=jnp.float32)
    mixed = mixed + jnp.dot(heads_narrow, out_narrow, preferred_element_type=jnp.float32)
    middle = (residual.astype(jnp.float32) + mixed).astype(jnp.bfloat16)
    middle_wide = middle.astype(jnp.float32)
    spread = jnp.mean(middle_wide * middle_wide, axis=1, keepdims=True)
    normed = (middle_wide * lax.rsqrt(spread + epsilon) * norm_gain).astype(jnp.bfloat16)
    features = normed.shape[1]
    chosen_count = routing.shape[1]
    expert_count = gate_weight.shape[0] * lax.axis_size("sp")
    capacity = own_rows * GROUPS // expert_count
    flat_routes = routing.reshape(-1)
    matches = (flat_routes[:, None] == jnp.arange(expert_count, dtype=jnp.int32)[None, :]).astype(
        jnp.int32
    )
    ranking = jnp.sum((jnp.cumsum(matches, axis=0) - matches) * matches, axis=1)
    placing = flat_routes * capacity + ranking
    picker = (
        placing[None, :] == jnp.arange(expert_count * capacity, dtype=jnp.int32)[:, None]
    ).astype(jnp.bfloat16)
    picker = jnp.sum(picker.reshape(expert_count * capacity, own_rows, chosen_count), axis=2)
    outgoing = jnp.dot(picker, normed, preferred_element_type=jnp.float32).astype(jnp.bfloat16)
    outgoing = outgoing.reshape(expert_count, capacity, features)
    arrived = lax.all_to_all(outgoing, "sp", split_axis=0, concat_axis=0, tiled=True)
    rows = arrived.reshape(-1, features)
    hidden = []
    for k in range(ny):
        gate_value = jnp.dot(rows, full_gate[k], preferred_element_type=jnp.float32)
        up_value = jnp.dot(rows, full_up[k], preferred_element_type=jnp.float32)
        hidden.append((jax.nn.silu(gate_value) * up_value).astype(jnp.bfloat16))
    hidden = jnp.concatenate(hidden, axis=1)
    answers = jnp.dot(hidden, full_down, preferred_element_type=jnp.float32).astype(jnp.bfloat16)
    returned = lax.all_to_all(
        answers.reshape(expert_count, capacity, features),
        "sp",
        split_axis=0,
        concat_axis=0,
        tiled=True,
    )
    picked = jnp.take(returned.reshape(expert_count * capacity, features), placing, axis=0)
    picked = picked.reshape(own_rows, chosen_count, features).astype(jnp.float32)
    combined = jnp.sum(route_weight[:, :, None] * picked, axis=1)
    return (middle_wide + combined).astype(jnp.bfloat16)


def solution(mesh):
    placed = (
        P(("sp", "tp"), None),
        P("sp", "tp"),
        P("sp", "tp"),
        P("sp", "tp"),
        P("sp", "tp"),
        P("sp", "tp"),
        P("sp", "tp"),
        P("sp", "tp"),
        P("sp", "tp"),
        P(),
        P(),
        P(),
        P(("sp", "tp"), None),
        P(("sp", "tp"), None),
        P("sp", None, "tp"),
        P("sp", None, "tp"),
        P("sp", "tp", None),
    )
    return jax.shard_map(
        body, mesh=mesh, in_specs=placed, out_specs=P(("sp", "tp"), None), check_vma=False
    )
```

time: 533 us -> 231 us (0.43)
  blocking collectives: 164 us -> 43.1 us
  local copies, waits for them, and re-layouts: 127 us -> 10.9 us
  waiting for transfers between devices: 161 us -> 66 us
  Pallas kernels: 0 us -> 54.1 us
  starting transfers between devices: 18.5 us -> 11.1 us
  other arithmetic: 16.4 us -> 9.23 us
  loops' own time: 6.28 us -> 0 us
    dynamic_slice x58 -> x0, local copies, waits for them, and re-layouts: 73.7 us -> none  [the longest x32 51.8 us: take_block(): return lax.dynamic_slice_in_dim(source, inside, block_size, 0)]
    all_to_all x1, blocking collectives: 116 us -> 43.1 us  [body(): lax.all_to_all(outgoing, 'sp', split_axis=0, concat_axis=0, tiled=True)]
    pallas_call x0 -> x1, Pallas kernels: none -> 54.1 us  [attend(): pl.pallas_call(functools.partial(attention_kernel, dims), out_shape=jax.S...]
    reduce_scatter x1 -> x0, waiting for transfers between devices: 50 us -> none  [body(): lax.psum_scatter(jnp.dot(hidden, down_weight[0], preferred_element_type=j...]
    all_gather x1 -> x0, blocking collectives: 48.7 us -> none  [sent_together(): whole, at, outs = (lax.all_gather(both, axis, axis=dim, tiled=True), 0, [])]
    all_gather x2 -> x3, waiting for transfers between devices: 77.8 us -> 36.3 us  [the longest x1 36.3 us: body(): full_down = lax.all_gather(down_weight[0], 'tp', axis=0, tiled=True)]
    slice x7 -> x2, local copies, waits for them, and re-layouts: 18.9 us -> 0.18 us  [the longest x4 17.3 us: sent_together(): outs.append(lax.slice_in_dim(whole, at, at + a.shape[along], axis=along))]
    reshape x2 -> x3, local copies, waits for them, and re-layouts: 10.3 us -> 1.18 us  [the longest x1 1.15 us: body(): rows = arrived.reshape(-1, features)]
  transfers between devices with their start and end apart: 6 -> 4, of which waited for: 6 -> 2; matrix products, arithmetic and copies ran while one was open for 6% -> 12% of each run, Pallas kernels for 0% -> 23%
where the time goes in v1:
time: 231 us; the launch traced here: 230 us
  waiting for transfers between devices  66 us (29%)
  Pallas kernels  54.1 us (23%)
  blocking collectives  43.1 us (19%)
  matrix products  22.5 us (10%)
  between operations  13.4 us (6%)
  starting transfers between devices  11.1 us (5%)
  local copies, waits for them, and re-layouts  10.9 us (5%)
  other arithmetic  9.23 us (4%)
    pallas_call x1, Pallas kernels, attend(): pl.pallas_call(functools.partial(attention_kernel, dims), out_shape=jax.S...  54.1 us
    all_to_all x1, blocking collectives, body(): lax.all_to_all(outgoing, 'sp', split_axis=0, concat_axis=0, tiled=True)  43.1 us
    all_gather x1, waiting for transfers between devices, body(): full_down = lax.all_gather(down_weight[0], 'tp', axis=0, tiled=True)  36.3 us
    all_to_all x1, waiting for transfers between devices, body(): lax.all_to_all(answers.reshape(expert_count, capacity, features), 'sp', s...  27.6 us
    all_to_all x1, starting transfers between devices, body(): lax.all_to_all(answers.reshape(expert_count, capacity, features), 'sp', s...  11 us
    dot_general x4, matrix products, body(): gate_value = jnp.dot(rows, full_gate[k], preferred_element_type=jnp.float32)  9.8 us
    dot_general x4, matrix products, body(): up_value = jnp.dot(rows, full_up[k], preferred_element_type=jnp.float32)  7.41 us
  transfers between devices with their start and end apart: 4, of which 2 were waited for; matrix products, arithmetic and copies ran while one was open for 12% of the time, Pallas kernels for 23%

profile of v1, /device:TPU:1, one launch (start us, length us, event | category | flops | bytes accessed | tf_op | source)
XLA Modules:
  0.0 230.4 jit_solution(16979588511638191365)
XLA Ops:
  6.5 0.0 copy-start
  6.5 0.0 all-gather.5.cloned.1.call-start
  6.5 0.7 all-gather.5.cloned.1.call-update
  7.3 0.0 all-gather.7.cloned.1.call-start
  7.3 0.7 all-gather.7.cloned.1.call-update
  8.0 0.0 all-gather.9.cloned.1.call-start
  8.1 0.7 all-gather.9.cloned.1.call-update
  8.7 0.7 fusion.37
  9.5 0.9 reduce-window.6
  10.4 0.1 slice.54
  10.5 0.1 copy.54
  10.6 0.1 copy.55
  10.7 0.1 add_multiply_fusion
  10.8 0.1 copy.65
  11.0 0.8 copy.61
  11.8 0.1 reshape.163
  12.0 0.1 fusion.34
  12.1 0.2 reduce_window_sum.41
  12.2 0.2 select_reduce_fusion
  12.4 0.1 reduce_sum.44
  12.6 0.1 copy.62
  12.6 0.7 compare_and_fusion
  13.3 0.1 fusion.28
  13.4 0.9 fusion.26.kd_ref
  14.3 1.0 pad_maximum_fusion
  15.3 0.0 copy-start.2
  15.3 0.0 copy-start.4
  15.3 54.1 %attend.1 = bf16[4,64,256]{2,1,0:T(8,128)(2,1)S(1)} custom-call(bf16[256,256]{1,0:T(8,128)(2,1)S(1)} %get-tuple-element.14.q_ref, bf16[272,256]{1,0:T(8,128)(2,1)S(1)} %fusion.26.kd_ref, bf16[256,256]{1,0:T(8,128)(2,1)S(1)} %get-tuple-element.15.v_ref, f32[1,128]{1,0:T(1,128)S(1)} %pad_bitcast_fusion.tot_ref), custom_call_target="tpu_custom_call" | custom-call | flops 10000000000 | bytes 10000000 | tf_op jit(solution)/shard_map/attend/pallas_call | solution.py:355
  69.4 0.0 copy-start.6
  69.4 0.0 copy-done.2
  69.4 0.5 fusion.31
  70.0 0.6 multiply_reduce_fusion.1
  70.6 0.8 copy-done.1
  71.4 0.5 convolution_convert_fusion
  71.9 1.2 reshape.164
  73.1 43.1 %all_to_all.10 = bf16[64,4,2048]{2,1,0:T(4,128)(2,1)S(1)} all-to-all(bf16[64,4,2048]{2,1,0:T(4,128)(2,1)} %reshape.164), channel_id=1, replica_groups=mesh['sp'=64,'tp'=4] {'sp'}, dimensions={0} | all-to-all | bytes 2097152 | tf_op jit(solution)/shard_map/all_to_all | solution.py:456
  116.2 1.1 reshape.165
  117.4 2.8 %fusion.15 = f32[256,256]{0,1:T(8,128)} fusion(bf16[256,2048]{1,0:T(8,128)(2,1)} %reshape.165, bf16[4,2048,256]{2,1,0:T(8,128)(2,1)} %all-gather.5.cloned.1.call-done), kind=kOutput, calls=%fused_computation.28 | convolution fusion | flops 268435456 | bytes 2359296 | tf_op jit(solution)/shard_map/dot_general | solution.py:460
  120.2 2.8 %fusion.14 = f32[256,256]{0,1:T(8,128)} fusion(bf16[256,2048]{1,0:T(8,128)(2,1)} %reshape.165, bf16[4,2048,256]{2,1,0:T(8,128)(2,1)} %all-gather.5.cloned.1.call-done), kind=kOutput, calls=%fused_computation.25 | convolution fusion | flops 268435456 | bytes 2359296 | tf_op jit(solution)/shard_map/dot_general | solution.py:460
  123.0 0.0 copy-done.3
  123.0 2.5 %fusion.13 = f32[256,256]{0,1:T(8,128)} fusion(bf16[256,2048]{1,0:T(8,128)(2,1)S(1)} %copy-done.3, bf16[4,2048,256]{2,1,0:T(8,128)(2,1)} %all-gather.5.cloned.1.call-done), kind=kOutput, calls=%fused_computation.22 | convolution fusion | flops 268435456 | bytes 2359296 | tf_op jit(solution)/shard_map/dot_general | solution.py:460
  125.4 1.7 fusion.12
  127.2 0.0 all-gather.7.cloned.1.call-done
  127.2 0.0 copy-start.9
  127.2 2.6 %fusion.8 = bf16[256,256]{0,1:T(8,128)(2,1)} fusion(bf16[256,2048]{1,0:T(8,128)(2,1)S(1)} %copy-done.3, bf16[4,2048,256]{2,1,0:T(8,128)(2,1)} %all-gather.7.cloned.1.call-done, f32[256,256]{0,1:T(8,128)} %fusion.15), kind=kOutput, calls=%fused_computation.13 | convolution fusion | flops 268828672 | bytes 2490368 | tf_op jit(solution)/shard_map/dot_general | solution.py:461
  129.8 2.4 %fusion.9 = bf16[256,256]{0,1:T(8,128)(2,1)} fusion(bf16[256,2048]{1,0:T(8,128)(2,1)S(1)} %copy-done.3, bf16[4,2048,256]{2,1,0:T(8,128)(2,1)} %all-gather.7.cloned.1.call-done, f32[256,256]{0,1:T(8,128)} %fusion.14), kind=kOutput, calls=%fused_computation.14 | convolution fusion | flops 268828672 | bytes 2490368 | tf_op jit(solution)/shard_map/dot_general | solution.py:461
  132.3 0.0 copy-done.9
  132.3 1.2 fusion.10
  133.4 1.2 fusion.11
  134.6 36.3 %all-gather.9.cloned.1.call-done = bf16[1,1024,2048]{2,1,0:T(8,128)(2,1)} async-done(((bf16[1,256,2048]{2,1,0:T(8,128)(2,1)}), bf16[1,1024,2048]{2,1,0:T(8,128)(2,1)}) %all-gather.9.cloned.1.call-update) | async-done | bytes 4194320 | tf_op jit(solution)/shard_map/all_gather | solution.py:425
  170.9 3.7 %fusion.2 = bf16[256,2048]{1,0:T(8,128)(2,1)S(1)} fusion(bf16[1,1024,2048]{2,1,0:T(8,128)(2,1)} %all-gather.9.cloned.1.call-done, bf16[256,256]{0,1:T(8,128)(2,1)} %fusion.11, bf16[256,256]{0,1:T(8,128)(2,1)} %fusion.10, bf16[256,256]{0,1:T(8,128)(2,1)} %fusion.9, bf16[256,256]{0,1:T(8,128)(2,1)} %fusion.8), kind=kOutput, calls=%fused_computation.3 | convolution fusion | flops 1076363264 | bytes 5767168 | tf_op jit(solution)/shard_map/dot_general | solution.py:464
  174.7 1.2 reshape.166
  175.9 11.0 %all-to-all-start.1 = ((bf16[64,4,2048]{2,1,0:T(4,128)(2,1)}), bf16[64,4,2048]{2,1,0:T(4,128)(2,1)}, u32[]{:S(2)}, u32[]{:S(2)}) async-start(bf16[64,4,2048]{2,1,0:T(4,128)(2,1)} %reshape.166), calls=%async_computation.1 | async-start | bytes 2097152 | tf_op jit(solution)/shard_map/all_to_all | solution.py:465
  187.0 0.1 copy.64
  187.1 0.1 mul.126
  187.2 0.1 copy.63
  187.3 0.0 copy-done.7
  187.3 0.1 copy.60
  187.4 27.6 %all-to-all-done.1 = bf16[64,4,2048]{2,1,0:T(4,128)(2,1)} async-done(((bf16[64,4,2048]{2,1,0:T(4,128)(2,1)}), bf16[64,4,2048]{2,1,0:T(4,128)(2,1)}, u32[]{:S(2)}, u32[]{:S(2)}) %all-to-all-start.1) | async-done | bytes 1048608 | tf_op jit(solution)/shard_map/all_to_all | solution.py:465
  215.0 1.3 reshape.167
  216.4 1.7 gather_fusion
  218.1 1.4 gather.7
  219.5 2.5 %multiply_reduce_fusion = f32[64,2048]{1,0:T(8,128)S(1)} fusion(bf16[64,2,2048]{2,1,0:T(2,128)(2,1)S(1)} %gather.7, pred[64,2]{1,0:T(8,128)(4,1)S(1)} %copy.63, f32[64,2]{1,0:T(8,128)S(1)} %copy.60), kind=kLoop, calls=%fused_computation.29 | loop fusion | flops 917504 | bytes 1049216 | tf_op jit(solution)/shard_map/reduce_sum | solution.py:474
  222.0 1.8 add_convert_fusion
  (26 shorter events, 0.2 us)
Async XLA Ops:
  6.5 63.4 %copy-start = (bf16[512,2048]{1,0:T(8,128)(2,1)S(1)}, bf16[512,2048]{1,0:T(8,128)(2,1)}, u32[]{:S(2)}) copy-start(bf16[512,2048]{1,0:T(8,128)(2,1)} %param.27) | copy-start | bytes 6291460
  6.5 110.8 %all-gather.5.cloned.1.call-start = ((), (), s32[]{:S(2)}) async-start(), calls=%async_computation.2 | async-start | bytes 5242880 | tf_op jit(solution)/shard_map/all_gather | solution.py:423
  7.3 119.9 %all-gather.7.cloned.1.call-start = ((), (), s32[]{:S(2)}) async-start(), calls=%async_computation.3 | async-start | bytes 5242880 | tf_op jit(solution)/shard_map/all_gather | solution.py:424
  8.0 162.9 %all-gather.9.cloned.1.call-start = ((), (), s32[]{:S(2)}) async-start(), calls=%async_computation.4 | async-start | bytes 5242880 | tf_op jit(solution)/shard_map/all_gather | solution.py:425
  15.3 54.2 %copy-start.2 = (bf16[512,2048]{1,0:T(8,128)(2,1)S(1)}, bf16[512,2048]{1,0:T(8,128)(2,1)}, u32[]{:S(2)}) copy-start(bf16[512,2048]{1,0:T(8,128)(2,1)} %param.26) | copy-start | bytes 6291460
  15.3 54.6 %copy-start.4 = (bf16[64,2048]{1,0:T(8,128)(2,1)S(1)}, bf16[64,2048]{1,0:T(8,128)(2,1)}, u32[]{:S(2)}) copy-start(bf16[64,2048]{1,0:T(8,128)(2,1)} %param.17) | copy-start | bytes 786436
  69.4 2.0 copy-start.6
  70.6 0.8 copy-start.1
  117.4 5.6 %copy-start.3 = (bf16[256,2048]{1,0:T(8,128)(2,1)S(1)}, bf16[256,2048]{1,0:T(8,128)(2,1)}, u32[]{:S(2)}) copy-start(bf16[256,2048]{1,0:T(8,128)(2,1)} %reshape.165) | copy-start | bytes 3145732
  127.2 5.1 %copy-start.8 = (bf16[4,2048,256]{2,1,0:T(8,128)(2,1)S(1)}, bf16[4,2048,256]{2,1,0:T(8,128)(2,1)}, u32[]{:S(2)}) copy-start(bf16[4,2048,256]{2,1,0:T(8,128)(2,1)} %all-gather.7.cloned.1.call-done) | copy-start | bytes 12582916
  127.2 5.0 %copy-start.9 = (f32[256,256]{0,1:T(8,128)S(1)}, f32[256,256]{0,1:T(8,128)}, u32[]{:S(2)}) copy-start(f32[256,256]{0,1:T(8,128)} %fusion.13) | copy-start | bytes 786436
  134.6 52.3 %copy-start.5 = (s32[64,2]{0,1:T(2,128)S(1)}, s32[64,2]{0,1:T(2,128)}, u32[]{:S(2)}) copy-start(s32[64,2]{0,1:T(2,128)} %param.29) | copy-start | bytes 1540
  134.6 52.7 %copy-start.7 = (f32[64,2]{0,1:T(2,128)S(1)}, f32[64,2]{0,1:T(2,128)}, u32[]{:S(2)}) copy-start(f32[64,2]{0,1:T(2,128)} %param.30) | copy-start | bytes 1540
  175.9 39.1 %all-to-all-start.1 = ((bf16[64,4,2048]{2,1,0:T(4,128)(2,1)}), bf16[64,4,2048]{2,1,0:T(4,128)(2,1)}, u32[]{:S(2)}, u32[]{:S(2)}) async-start(bf16[64,4,2048]{2,1,0:T(4,128)(2,1)} %reshape.166), calls=%async_computation.1 | async-start | bytes 2097152 | tf_op jit(solution)/shard_map/all_to_all | solution.py:465
Sparse Core Ops, SparseCore 0:
  9.1 54.4 all-gather.4
  65.4 52.5 all-gather.6
  119.8 51.1 all-gather.8

commit v2 on v1

--- a/solution.py
+++ b/solution.py
@@ -12,16 +12,16 @@
 F32, BF16 = jnp.float32, jnp.bfloat16
 HW = 128
 HN = 64
-GROUPS = 4
+NX = 4
 LOG2E = math.log2(math.e)
 NEG = -1e30
 epsilon = 1e-06
 
 
 def attention_kernel(
-    dims, q_ref, kd_ref, v_ref, tot_ref, att_ref,
+    dims, q_ref, kd_ref, v_ref, tot_ref, gate_ref, up_ref, att_ref, peer_gate, peer_up,
     qb, kb, vb, tt, drow, mb, acc, ob, sb, orv, srv, ab, ar,
-    q_s, q_r, up_s, up_r, dn_s, dn_r, pr_s, pr_r, t1_s, t1_r, t2_s, t2_r, o_s, o_r, y_s, y_r, loc,
+    q_s, q_r, up_s, up_r, dn_s, dn_r, pr_s, pr_r, t1_s, t1_r, t2_s, t2_r, o_s, o_r, y_s, y_r, loc, w_s, w_r,
 ):
     nz, nx, ny = dims
     half = nz // 2
@@ -118,6 +118,14 @@
         q_copy(i).start()
     for j in range(2):
         own_pr(j).start()
+    pair = at(z, x, c, lax.rem(y, 2) * (y - 1) + (1 - lax.rem(y, 2)) * (y + 1))
+    first_rows = pl.ds(0, peer_up.shape[0])
+    weights = [
+        remote(gate_ref, peer_gate, w_s.at[0], w_r.at[0], pair),
+        remote(up_ref.at[first_rows, :], peer_up, w_s.at[1], w_r.at[1], pair),
+    ]
+    for copy in weights:
+        copy.start()
     local = [
         pltpu.make_async_copy(tot_ref, tt.at[z, xc], loc.at[0]),
         pltpu.make_async_copy(q_ref, qb.at[x], loc.at[1]),
@@ -320,6 +328,8 @@
         remote(rows_of(src), ar.at[src], y_s.at[i - 1], y_r.at[i - 1], at(z, x, c, src)).wait_recv()
         att_ref[src] = ar[src]
 
+    for copy in weights:
+        copy.wait()
     for j in range(2):
         if up_has(1, j):
             own_up(j).wait_send()
@@ -347,16 +357,21 @@
         y_copy(i).wait_send()
 
 
-def attend(dims, q, kd, v, tot):
+def attend(dims, q, kd, v, tot, gate, up):
     nz, nx, ny = dims
     half = nz // 2
     dma = pltpu.SemaphoreType.DMA
     vmem = pl.BlockSpec(memory_space=pltpu.VMEM)
+    hbm = pl.BlockSpec(memory_space=pl.ANY)
     return pl.pallas_call(
         functools.partial(attention_kernel, dims),
-        out_shape=jax.ShapeDtypeStruct((ny, 256 // ny, 256), BF16),
-        in_specs=[vmem] * 4,
-        out_specs=vmem,
+        out_shape=[
+            jax.ShapeDtypeStruct((ny, 256 // ny, 256), BF16),
+            jax.ShapeDtypeStruct(gate.shape, BF16),
+            jax.ShapeDtypeStruct((up.shape[0] // 2, up.shape[1]), BF16),
+        ],
+        in_specs=[vmem] * 4 + [hbm] * 2,
+        out_specs=[vmem, hbm, hbm],
         scratch_shapes=[
             pltpu.VMEM((nx, 256, 256), BF16),
             pltpu.VMEM((nz, 2, 272, 256), BF16),
@@ -375,12 +390,12 @@
             dma((half + 1, 2)), dma((half + 1, 2)), dma((half + 1, 2)), dma((half + 1, 2)),
             dma((nz, 2)), dma((nz, 2)),
             dma((2 * nx,)), dma((2 * nx,)), dma((nz,)), dma((nz,)),
-            dma((nx, 2)), dma((nx, 2)), dma((ny,)), dma((ny,)), dma((4,)),
+            dma((nx, 2)), dma((nx, 2)), dma((ny,)), dma((ny,)), dma((4,)), dma((2,)), dma((2,)),
         ],
         compiler_params=pltpu.CompilerParams(collective_id=1, has_side_effects=True, vmem_limit_bytes=40 * 2**20),
         cost_estimate=pl.CostEstimate(flops=10**10, bytes_accessed=10**7, transcendentals=12 * 10**6),
         name="attend",
-    )(q, kd, v, tot)
+    )(q, kd, v, tot, gate, up)
 
 
 def prepare(query_wide, key_wide, value_wide, query_narrow, key_narrow, value_narrow, gate_wide, gate_narrow):
@@ -395,6 +410,364 @@
     kd = jnp.concatenate([jnp.concatenate([key_wide, key_narrow], axis=1), parts], axis=0)
     v = jnp.concatenate([value_wide, value_narrow], axis=1)
     return q, kd, v, tot
+
+
+def paired(y):
+    return lax.rem(y, 2) * (y - 1) + (1 - lax.rem(y, 2)) * (y + 1)
+
+
+def plane_at(t, z, nz):
+    d = jnp.where(lax.rem(t, 2) == 1, (t + 1) // 2, nz - t // 2)
+    return lax.rem(z + d, nz)
+
+
+def to_rows(take, tmp, plane):
+    for k in range(plane // 2):
+        tmp[8 * k:8 * k + 8, :] = jnp.concatenate([take(2 * k).astype(F32), take(2 * k + 1).astype(F32)], axis=0)
+
+
+def dispatch_kernel(
+    dims, att_ref, res_ref, wide_ref, narrow_ref, gain_ref, picker_ref, up_ref, down_ref,
+    own_ref, cross_ref, mid_ref, peer_up, peer_down,
+    ow, on, perm, tmp, snd, arr, arc, a_s, a_r, c_s, c_r, w_s, w_r, loc,
+):
+    nz, nx, ny = dims
+    plane = 2 * nx
+    count = nz * plane
+    sp, y = lax.axis_index("sp"), lax.axis_index("tp")
+    z = sp // plane
+    fetch = [pltpu.make_async_copy(wide_ref, ow, loc.at[0]), pltpu.make_async_copy(narrow_ref, on, loc.at[1])]
+    for copy in fetch:
+        copy.start()
+
+    def remote(src, dst, send, recv, device):
+        return pltpu.make_async_remote_copy(
+            src_ref=src, dst_ref=dst, send_sem=send, recv_sem=recv, device_id=device, device_id_type=MESH
+        )
+
+    barrier = pltpu.get_barrier_semaphore()
+    pair, across = (sp, paired(y)), (sp, ny - 1 - y)
+
+    def greet(i, carry):
+        pl.semaphore_signal(barrier, inc=1, device_id=(lax.rem(sp + i, count), y), device_id_type=MESH)
+        return carry
+    lax.fori_loop(1, count, greet, 0)
+    pl.semaphore_signal(barrier, inc=1, device_id=pair, device_id_type=MESH)
+    pl.semaphore_signal(barrier, inc=1, device_id=across, device_id_type=MESH)
+
+    done = up_ref.shape[0] - peer_up.shape[0]
+    for copy in fetch:
+        copy.wait()
+    a_wide = jnp.concatenate([att_ref[k, :, :128] for k in range(ny)], axis=1)
+    a_narrow = jnp.concatenate([att_ref[k, :, 128:] for k in range(ny)], axis=1)
+    mixed = jnp.dot(a_wide, ow[...], preferred_element_type=F32) + jnp.dot(a_narrow, on[...], preferred_element_type=F32)
+    middle = (res_ref[...].astype(F32) + mixed).astype(BF16)
+    mid_ref[...] = middle
+    middle = middle.astype(F32)
+    spread = jnp.mean(middle * middle, axis=1, keepdims=True)
+    normed = (middle * lax.rsqrt(spread + epsilon) * gain_ref[...]).astype(BF16)
+    perm[...] = jnp.dot(picker_ref[...], normed, preferred_element_type=F32)
+
+    def cut(k, carry):
+        v = perm[pl.ds(pl.multiple_of(8 * k, 8), 8), :]
+        snd[2 * k] = v[:4].astype(BF16)
+        snd[2 * k + 1] = v[4:].astype(BF16)
+        return carry
+    lax.fori_loop(0, count // 2, cut, 0)
+
+    pl.semaphore_wait(barrier, count - 1 + 2)
+    weights = [
+        remote(up_ref.at[pl.ds(done, peer_up.shape[0]), :], peer_up, w_s.at[0], w_r.at[0], pair),
+        remote(down_ref, peer_down, w_s.at[1], w_r.at[1], pair),
+    ]
+    for copy in weights:
+        copy.start()
+
+    def out_copy(e):
+        return remote(snd.at[e], arr.at[sp], a_s.at[e], a_r.at[sp], (e, y))
+
+    keep = pltpu.make_async_copy(snd.at[sp], arr.at[sp], loc.at[2])
+    keep.start()
+
+    def send(t, carry):
+        first = plane_at(t, z, nz) * plane
+
+        def one(k, inner):
+            e = first + k
+
+            @pl.when(e != sp)
+            def _():
+                out_copy(e).start()
+            return inner
+        return lax.fori_loop(0, plane, one, carry)
+    lax.fori_loop(0, nz, send, 0)
+    keep.wait()
+
+    def cross_copy(p):
+        part = pl.ds(p * plane, plane)
+        return remote(arr.at[part], arc.at[part], c_s.at[p], c_r.at[p], across)
+
+    def arrive(t, carry):
+        p = plane_at(t, z, nz)
+        first = p * plane
+
+        def one(k, inner):
+            s = first + k
+
+            @pl.when(s != sp)
+            def _():
+                remote(snd.at[s], arr.at[s], a_s.at[s], a_r.at[s], (s, y)).wait_recv()
+            return inner
+        lax.fori_loop(0, plane, one, 0)
+        cross_copy(p).start()
+        to_rows(lambda k: arr[first + k], tmp, plane)
+        own_ref[pl.ds(pl.multiple_of(first * 4, 4 * plane), 4 * plane), :] = tmp[...].astype(BF16)
+        return carry
+    lax.fori_loop(0, nz, arrive, 0)
+
+    def arrive_cross(t, carry):
+        p = plane_at(t, z, nz)
+        first = p * plane
+        cross_copy(p).wait_recv()
+        to_rows(lambda k: arc[first + k], tmp, plane)
+        cross_ref[pl.ds(pl.multiple_of(first * 4, 4 * plane), 4 * plane), :] = tmp[...].astype(BF16)
+        return carry
+    lax.fori_loop(0, nz, arrive_cross, 0)
+
+    def drain(e, carry):
+        @pl.when(e != sp)
+        def _():
+            out_copy(e).wait_send()
+        return carry
+    lax.fori_loop(0, count, drain, 0)
+
+    def drain_cross(p, carry):
+        cross_copy(p).wait_send()
+        return carry
+    lax.fori_loop(0, nz, drain_cross, 0)
+    for copy in weights:
+        copy.wait()
+
+
+def dispatch(dims, att, residual, wide, narrow, gain, picker, up, down):
+    nz, nx, ny = dims
+    count, features = nz * nx * 2, residual.shape[1]
+    dma = pltpu.SemaphoreType.DMA
+    vmem = pl.BlockSpec(memory_space=pltpu.VMEM)
+    hbm = pl.BlockSpec(memory_space=pl.ANY)
+    shape = jax.ShapeDtypeStruct
+    return pl.pallas_call(
+        functools.partial(dispatch_kernel, dims),
+        out_shape=[
+            shape((4 * count, features), BF16),
+            shape((4 * count, features), BF16),
+            shape(residual.shape, BF16),
+            shape((up.shape[0] // 2, up.shape[1]), BF16),
+            shape(down.shape, BF16),
+        ],
+        in_specs=[vmem, vmem, hbm, hbm, vmem, vmem, hbm, hbm],
+        out_specs=[vmem, vmem, vmem, hbm, hbm],
+        scratch_shapes=[
+            pltpu.VMEM(wide.shape, BF16),
+            pltpu.VMEM(narrow.shape, BF16),
+            pltpu.VMEM((4 * count, features), F32),
+            pltpu.VMEM((8 * nx, features), F32),
+            pltpu.VMEM((count, 4, features), BF16),
+            pltpu.VMEM((count, 4, features), BF16),
+            pltpu.VMEM((count, 4, features), BF16),
+            dma((count,)), dma((count,)), dma((nz,)), dma((nz,)), dma((2,)), dma((2,)), dma((3,)),
+        ],
+        compiler_params=pltpu.CompilerParams(collective_id=2, has_side_effects=True, vmem_limit_bytes=40 * 2**20),
+        cost_estimate=pl.CostEstimate(flops=10**9, bytes_accessed=10**7, transcendentals=1000),
+        name="dispatch",
+    )(att, residual, wide, narrow, gain, picker, up, down)
+
+
+def expert_kernel(
+    dims, own_ref, cross_ref, gate_ref, up_ref, down_ref, peer_gate, peer_up0, peer_up1, peer_down, mid_ref, share_ref,
+    out_ref,
+    wg, wu, wd, total, part, back, tmp, snd, ret, rows, p_s, p_r, b_s, b_r, loc,
+):
+    nz, nx, ny = dims
+    plane = 2 * nx
+    count = nz * plane
+    sp, y = lax.axis_index("sp"), lax.axis_index("tp")
+    z = sp // plane
+    half = peer_up0.shape[0]
+    fetch = [
+        pltpu.make_async_copy(gate_ref, wg.at[0], loc.at[0]),
+        pltpu.make_async_copy(peer_gate, wg.at[1], loc.at[1]),
+        pltpu.make_async_copy(up_ref, wu.at[0], loc.at[2]),
+        pltpu.make_async_copy(peer_up0, wu.at[1, pl.ds(0, half), :], loc.at[3]),
+        pltpu.make_async_copy(peer_up1, wu.at[1, pl.ds(half, half), :], loc.at[4]),
+        pltpu.make_async_copy(down_ref, wd.at[0], loc.at[5]),
+        pltpu.make_async_copy(peer_down, wd.at[1], loc.at[6]),
+    ]
+    for copy in fetch:
+        copy.start()
+
+    def remote(src, dst, send, recv, device):
+        return pltpu.make_async_remote_copy(
+            src_ref=src, dst_ref=dst, send_sem=send, recv_sem=recv, device_id=device, device_id_type=MESH
+        )
+
+    barrier = pltpu.get_barrier_semaphore()
+    across = (sp, ny - 1 - y)
+
+    def greet(i, carry):
+        pl.semaphore_signal(barrier, inc=1, device_id=(lax.rem(sp + i, count), y), device_id_type=MESH)
+        return carry
+    lax.fori_loop(1, count, greet, 0)
+    pl.semaphore_signal(barrier, inc=1, device_id=across, device_id_type=MESH)
+    for copy in fetch[:5]:
+        copy.wait()
+
+    def hidden(x):
+        both = []
+        for k in range(2):
+            g = jnp.dot(x, wg[k], preferred_element_type=F32)
+            u = jnp.dot(x, wu[k], preferred_element_type=F32)
+            both.append((jax.nn.silu(g) * u).astype(BF16))
+        return both
+
+    def down(h, put):
+        step = 512
+        for q in range(wd.shape[2] // step):
+            cols = slice(q * step, (q + 1) * step)
+            put(
+                cols,
+                jnp.dot(h[0], wd[0, :, cols], preferred_element_type=F32)
+                + jnp.dot(h[1], wd[1, :, cols], preferred_element_type=F32),
+            )
+
+    h = hidden(cross_ref[...])
+    for copy in fetch[5:]:
+        copy.wait()
+
+    def put_part(cols, value):
+        part[:, cols] = value.astype(BF16)
+    down(h, put_part)
+    pl.semaphore_wait(barrier, count)
+
+    def rows_of(ref, p):
+        return ref.at[pl.ds(pl.multiple_of(p * 4 * plane, 4 * plane), 4 * plane), :]
+
+    def part_copy(p):
+        return remote(rows_of(part, p), rows_of(back, p), p_s.at[p], p_r.at[p], across)
+
+    def send_part(t, carry):
+        part_copy(plane_at(t, z, nz)).start()
+        return carry
+    lax.fori_loop(0, nz, send_part, 0)
+
+    h = hidden(own_ref[...])
+
+    def put_total(cols, value):
+        total[:, cols] = value
+    down(h, put_total)
+
+    def back_copy(e):
+        return remote(snd.at[e], ret.at[sp], b_s.at[e], b_r.at[sp], (e, y))
+
+    def finish(t, carry):
+        p = plane_at(t, z, nz)
+        first = p * plane
+        part_copy(p).wait_recv()
+        some = pl.ds(pl.multiple_of(first * 4, 4 * plane), 4 * plane)
+        tmp[...] = total[some, :] + back[some, :].astype(F32)
+        for k in range(plane // 2):
+            v = tmp[8 * k:8 * k + 8, :]
+            snd[first + 2 * k] = v[:4].astype(BF16)
+            snd[first + 2 * k + 1] = v[4:].astype(BF16)
+
+        def one(k, inner):
+            e = first + k
+
+            @pl.when(e != sp)
+            def _():
+                back_copy(e).start()
+            return inner
+        return lax.fori_loop(0, plane, one, carry)
+    lax.fori_loop(0, nz, finish, 0)
+    keep = pltpu.make_async_copy(snd.at[sp], ret.at[sp], loc.at[7])
+    keep.start()
+    keep.wait()
+
+    def arrive(t, carry):
+        first = plane_at(t, z, nz) * plane
+
+        def one(k, inner):
+            e = first + k
+
+            @pl.when(e != sp)
+            def _():
+                remote(snd.at[e], ret.at[e], b_s.at[e], b_r.at[e], (e, y)).wait_recv()
+            return inner
+        lax.fori_loop(0, plane, one, 0)
+        to_rows(lambda k: ret[first + k], tmp, plane)
+        rows[pl.ds(pl.multiple_of(first * 4, 4 * plane), 4 * plane), :] = tmp[...].astype(BF16)
+        return carry
+    lax.fori_loop(0, nz, arrive, 0)
+    combined = mid_ref[...].astype(F32)
+    for k in range(3):
+        combined = combined + jnp.dot(share_ref[k], rows[...], preferred_element_type=F32)
+    out_ref[...] = combined.astype(BF16)
+
+    def drain(e, carry):
+        @pl.when(e != sp)
+        def _():
+            back_copy(e).wait_send()
+        return carry
+    lax.fori_loop(0, count, drain, 0)
+
+    def drain_part(p, carry):
+        part_copy(p).wait_send()
+        return carry
+    lax.fori_loop(0, nz, drain_part, 0)
+
+
+def experts(dims, own, cross, gate, up, down, peer_gate, peer_up0, peer_up1, peer_down, middle, shares):
+    nz, nx, ny = dims
+    count, features = nz * nx * 2, middle.shape[1]
+    dma = pltpu.SemaphoreType.DMA
+    vmem = pl.BlockSpec(memory_space=pltpu.VMEM)
+    hbm = pl.BlockSpec(memory_space=pl.ANY)
+    return pl.pallas_call(
+        functools.partial(expert_kernel, dims),
+        out_shape=jax.ShapeDtypeStruct(middle.shape, BF16),
+        in_specs=[vmem] * 2 + [hbm] * 7 + [vmem] * 2,
+        out_specs=vmem,
+        scratch_shapes=[
+            pltpu.VMEM((2, *gate.shape), BF16),
+            pltpu.VMEM((2, *up.shape), BF16),
+            pltpu.VMEM((2, *down.shape), BF16),
+            pltpu.VMEM((4 * count, features), F32),
+            pltpu.VMEM((4 * count, features), BF16),
+            pltpu.VMEM((4 * count, features), BF16),
+            pltpu.VMEM((8 * nx, features), F32),
+            pltpu.VMEM((count, 4, features), BF16),
+            pltpu.VMEM((count, 4, features), BF16),
+            pltpu.VMEM((4 * count, features), BF16),
+            dma((nz,)), dma((nz,)), dma((count,)), dma((count,)), dma((8,)),
+        ],
+        compiler_params=pltpu.CompilerParams(collective_id=3, has_side_effects=True, vmem_limit_bytes=48 * 2**20),
+        cost_estimate=pl.CostEstimate(flops=10**9, bytes_accessed=10**7, transcendentals=1000),
+        name="experts",
+    )(own, cross, gate, up, down, peer_gate, peer_up0, peer_up1, peer_down, middle, shares)
+
+
+def tables(routing, route_weight, slots):
+    flat = routing.reshape(-1)
+    experts_here = jnp.arange(slots // 4, dtype=jnp.int32)
+    matches = (flat[:, None] == experts_here[None, :]).astype(jnp.int32)
+    ranking = jnp.sum((jnp.cumsum(matches, axis=0) - matches) * matches, axis=1)
+    placing = (flat * 4 + ranking).reshape(routing.shape)
+    hits = placing[:, :, None] == jnp.arange(slots, dtype=jnp.int32)[None, None, :]
+    picker = jnp.sum(hits.astype(F32), axis=1).T.astype(BF16)
+    shares = jnp.sum(jnp.where(hits, route_weight[:, :, None], 0.0), axis=1)
+    high = lax.reduce_precision(shares, 8, 7)
+    mid = lax.reduce_precision(shares - high, 8, 7)
+    return picker, jnp.stack([high, mid, shares - high - mid]).astype(BF16)
 
 
 def body(
@@ -417,62 +790,18 @@
     down_weight,
 ):
     ny = lax.axis_size("tp")
-    nx = 4
+    nx = NX
     dims = (lax.axis_size("sp") // (2 * nx), nx, ny)
-    own_rows = residual.shape[0]
-    full_gate = lax.all_gather(gate_weight[0], "tp", axis=0)
-    full_up = lax.all_gather(up_weight[0], "tp", axis=0)
-    full_down = lax.all_gather(down_weight[0], "tp", axis=0, tiled=True)
-    att = attend(
-        dims,
-        *prepare(
-            query_wide, key_wide, value_wide, query_narrow, key_narrow, value_narrow, gate_wide, gate_narrow
-        ),
+    gate, up, down = gate_weight[0], up_weight[0], down_weight[0]
+    picker, shares = tables(routing, route_weight, 4 * lax.axis_size("sp"))
+    ready = prepare(
+        query_wide, key_wide, value_wide, query_narrow, key_narrow, value_narrow, gate_wide, gate_narrow
     )
-    heads_wide = jnp.transpose(att[:, :, :128], (1, 0, 2)).reshape(own_rows, 128 * ny)
-    heads_narrow = jnp.transpose(att[:, :, 128:], (1, 0, 2)).reshape(own_rows, 128 * ny)
-    mixed = jnp.dot(heads_wide, out_wide, preferred_element_type=jnp.float32)
-    mixed = mixed + jnp.dot(heads_narrow, out_narrow, preferred_element_type=jnp.float32)
-    middle = (residual.astype(jnp.float32) + mixed).astype(jnp.bfloat16)
-    middle_wide = middle.astype(jnp.float32)
-    spread = jnp.mean(middle_wide * middle_wide, axis=1, keepdims=True)
-    normed = (middle_wide * lax.rsqrt(spread + epsilon) * norm_gain).astype(jnp.bfloat16)
-    features = normed.shape[1]
-    chosen_count = routing.shape[1]
-    expert_count = gate_weight.shape[0] * lax.axis_size("sp")
-    capacity = own_rows * GROUPS // expert_count
-    flat_routes = routing.reshape(-1)
-    matches = (flat_routes[:, None] == jnp.arange(expert_count, dtype=jnp.int32)[None, :]).astype(
-        jnp.int32
+    att, peer_gate, peer_up0 = attend(dims, *ready, gate, up)
+    own, cross, middle, peer_up1, peer_down = dispatch(
+        dims, att, residual, out_wide, out_narrow, norm_gain[None, :], picker, up, down
     )
-    ranking = jnp.sum((jnp.cumsum(matches, axis=0) - matches) * matches, axis=1)
-    placing = flat_routes * capacity + ranking
-    picker = (
-        placing[None, :] == jnp.arange(expert_count * capacity, dtype=jnp.int32)[:, None]
-    ).astype(jnp.bfloat16)
-    picker = jnp.sum(picker.reshape(expert_count * capacity, own_rows, chosen_count), axis=2)
-    outgoing = jnp.dot(picker, normed, preferred_element_type=jnp.float32).astype(jnp.bfloat16)
-    outgoing = outgoing.reshape(expert_count, capacity, features)
-    arrived = lax.all_to_all(outgoing, "sp", split_axis=0, concat_axis=0, tiled=True)
-    rows = arrived.reshape(-1, features)
-    hidden = []
-    for k in range(ny):
-        gate_value = jnp.dot(rows, full_gate[k], preferred_element_type=jnp.float32)
-        up_value = jnp.dot(rows, full_up[k], preferred_element_type=jnp.float32)
-        hidden.append((jax.nn.silu(gate_value) * up_value).astype(jnp.bfloat16))
-    hidden = jnp.concatenate(hidden, axis=1)
-    answers = jnp.dot(hidden, full_down, preferred_element_type=jnp.float32).astype(jnp.bfloat16)
-    returned = lax.all_to_all(
-        answers.reshape(expert_count, capacity, features),
-        "sp",
-        split_axis=0,
-        concat_axis=0,
-        tiled=True,
-    )
-    picked = jnp.take(returned.reshape(expert_count * capacity, features), placing, axis=0)
-    picked = picked.reshape(own_rows, chosen_count, features).astype(jnp.float32)
-    combined = jnp.sum(route_weight[:, :, None] * picked, axis=1)
-    return (middle_wide + combined).astype(jnp.bfloat16)
+    return experts(dims, own, cross, gate, up, down, peer_gate, peer_up0, peer_up1, peer_down, middle, shares)
 
 
 def solution(mesh):

time: 231 us -> 161 us (0.70)
  Pallas kernels: 54.1 us -> 147 us
  waiting for transfers between devices: 66 us -> 0 us
  blocking collectives: 43.1 us -> 0 us
  matrix products: 22.5 us -> 0 us
  between operations: 13.4 us -> 0.24 us
  starting transfers between devices: 11.1 us -> 0 us
  local copies, waits for them, and re-layouts: 10.9 us -> 5.92 us
  other arithmetic: 9.23 us -> 5.58 us
    pallas_call x1 -> x3, Pallas kernels: 54.1 us -> 147 us  [the longest x1 54.1 us: attend(): pl.pallas_call(functools.partial(attention_kernel, dims), out_shape=[jax....]
    all_to_all x1 -> x0, blocking collectives: 43.1 us -> none  [body(): lax.all_to_all(outgoing, 'sp', split_axis=0, concat_axis=0, tiled=True)]
    all_gather x3 -> x0, waiting for transfers between devices: 36.3 us -> none  [the longest x1 36.3 us: body(): full_down = lax.all_gather(down_weight[0], 'tp', axis=0, tiled=True)]
    all_to_all x1 -> x0, waiting for transfers between devices: 27.6 us -> none  [body(): lax.all_to_all(answers.reshape(expert_count, capacity, features), 'sp', s...]
    dot_general x12 -> x0, matrix products: 22.5 us -> none  [the longest x4 9.8 us: body(): gate_value = jnp.dot(rows, full_gate[k], preferred_element_type=jnp.float32)]
    all_to_all x1 -> x0, starting transfers between devices: 11 us -> none  [body(): lax.all_to_all(answers.reshape(expert_count, capacity, features), 'sp', s...]
    reshape x6 -> x1, local copies, waits for them, and re-layouts: 5.11 us -> 0.01 us  [the longest x1 1.33 us: body(): returned.reshape(expert_count * capacity, features)]
    unnamed x23 -> x24, local copies, waits for them, and re-layouts: 1.71 us -> 4.98 us
  transfers between devices with their start and end apart: 4 -> 0, of which waited for: 2 -> 0; matrix products, arithmetic and copies ran while one was open for 12% -> 0% of each run, Pallas kernels for 23% -> 0%
where the time goes in v2:
time: 161 us; the launch traced here: 158 us
  Pallas kernels  147 us (91%)
  local copies, waits for them, and re-layouts  5.92 us (4%)
  other arithmetic  5.58 us (3%)
    pallas_call x1, Pallas kernels, attend(): pl.pallas_call(functools.partial(attention_kernel, dims), out_shape=[jax....  54.1 us
    pallas_call x1, Pallas kernels, dispatch(): pl.pallas_call(functools.partial(dispatch_kernel, dims), out_shape=[shape...  49 us
    pallas_call x1, Pallas kernels, experts(): pl.pallas_call(functools.partial(expert_kernel, dims), out_shape=jax.Shap...  43.5 us
    unnamed x24, local copies, waits for them, and re-layouts  4.98 us

profile of v2, /device:TPU:1, one launch (start us, length us, event | category | flops | bytes accessed | tf_op | source)
XLA Modules:
  0.0 158.4 jit_solution(9885659850854170756)
XLA Ops:
  0.0 0.7 fusion.6
  0.7 0.9 reduce-window.6
  1.7 0.1 slice.12
  1.7 0.1 copy.44
  1.9 0.1 copy.45
  2.0 0.1 add_multiply_fusion
  2.1 0.8 copy.48
  2.9 0.1 eq.28
  3.0 0.1 fusion.3
  3.1 0.2 reduce_window_sum.41
  3.3 0.2 select_reduce_fusion.1
  3.5 0.1 reduce_sum.32
  3.6 0.1 copy.49
  3.7 0.7 multiply_add_fusion
  4.4 0.8 select_reduce_fusion
  5.2 0.1 copy.50
  5.4 0.1 copy.51
  5.5 0.9 fusion.1.kd_ref
  6.4 1.0 pad_maximum_fusion
  7.4 0.0 copy-start
  7.4 1.2 copy-done
  8.6 0.0 copy-start.5
  8.6 1.2 copy-done.5
  9.9 0.0 copy-start.1
  9.9 0.0 copy-start.2
  9.9 0.0 copy-start.3
  9.9 0.0 copy-start.4
  9.9 0.0 copy-start.9
  9.9 0.0 copy-start.10
  9.9 54.1 %attend.1 = (bf16[4,64,256]{2,1,0:T(8,128)(2,1)S(1)}, bf16[2048,256]{1,0:T(8,128)(2,1)S(1)}, bf16[1024,256]{1,0:T(8,128)(2,1)S(1)}) custom-call(bf16[256,256]{1,0:T(8,128)(2,1)S(1)} %get-tuple-element.29.q_ref, bf16[272,256]{1,0:T(8,128)(2,1)S(1)} %fusion.1.kd_ref, bf16[256,256]{1,0:T(8,128)(2,1)S(1)} %get-tuple-element.30.v_ref, ...), custom_call_target="tpu_custom_call" | custom-call | flops 10000000000 | bytes 10000000 | tf_op jit(solution)/shard_map/attend/pallas_call | solution.py:366
  64.0 0.0 copy-start.7
  64.0 0.0 copy-done.1
  64.0 0.0 copy-done.2
  64.1 0.0 copy-done.3
  64.1 0.0 copy-done.4
  64.1 0.0 copy-done.9
  64.1 0.0 copy-done.10
  64.1 0.0 copy-start.6
  64.1 49.0 %dispatch.1 = (bf16[256,2048]{1,0:T(8,128)(2,1)S(1)}, bf16[256,2048]{1,0:T(8,128)(2,1)S(1)}, bf16[64,2048]{1,0:T(8,128)(2,1)S(1)}, bf16[1024,256]{1,0:T(8,128)(2,1)S(1)}, bf16[256,2048]{1,0:T(8,128)(2,1)S(1)}) custom-call(bf16[4,64,256]{2,1,0:T(8,128)(2,1)S(1)} %get-tuple-element.13.att_ref, bf16[64,2048]{1,0:T(8,128)(2,1)S(1)} %copy-done.9, ...), custom_call_target="tpu_custom_call" | custom-call | flops 1000000000 | bytes 10000000 | tf_op jit(solution)/shard_map/dispatch/pallas_call | solution.py:559
  113.1 0.0 copy-done.7
  113.1 0.0 copy-start.8
  113.2 1.0 copy-done.8
  114.2 0.0 copy-done.6
  114.2 43.5 %experts.1 = bf16[64,2048]{1,0:T(8,128)(2,1)S(1)} custom-call(bf16[256,2048]{1,0:T(8,128)(2,1)S(1)} %get-tuple-element.14.own_ref, bf16[256,2048]{1,0:T(8,128)(2,1)S(1)} %get-tuple-element.15.cross_ref, bf16[2048,256]{1,0:T(8,128)(2,1)S(1)} %bitcast.26, bf16[2048,256]{1,0:T(8,128)(2,1)S(1)} %bitcast.22, bf16[256,2048]{1,0:T(8,128)(2,1)} %bitcast.23, ...), custom_call_target="tpu_custom_call" | custom-call | flops 1000000000 | bytes 10000000 | tf_op jit(solution)/shard_map/experts/pallas_call | solution.py:735
  157.7 0.7 copy.53
  (12 shorter events, 0.2 us)
Async XLA Ops:
  7.4 1.2 copy-start
  8.6 1.2 copy-start.5
  9.9 54.2 %copy-start.1 = (bf16[1,2048,256]{2,1,0:T(8,128)(2,1)S(1)}, bf16[1,2048,256]{2,1,0:T(8,128)(2,1)}, u32[]{:S(2)}) copy-start(bf16[1,2048,256]{2,1,0:T(8,128)(2,1)} %param.32) | copy-start | bytes 3145732
  9.9 54.2 %copy-start.2 = (bf16[1,256,2048]{2,1,0:T(8,128)(2,1)S(1)}, bf16[1,256,2048]{2,1,0:T(8,128)(2,1)}, u32[]{:S(2)}) copy-start(bf16[1,256,2048]{2,1,0:T(8,128)(2,1)} %param.33) | copy-start | bytes 3145732
  9.9 54.2 %copy-start.3 = (bf16[512,2048]{1,0:T(8,128)(2,1)S(1)}, bf16[512,2048]{1,0:T(8,128)(2,1)}, u32[]{:S(2)}) copy-start(bf16[512,2048]{1,0:T(8,128)(2,1)} %wide_ref.1) | copy-start | bytes 6291460
  9.9 54.2 %copy-start.4 = (bf16[512,2048]{1,0:T(8,128)(2,1)S(1)}, bf16[512,2048]{1,0:T(8,128)(2,1)}, u32[]{:S(2)}) copy-start(bf16[512,2048]{1,0:T(8,128)(2,1)} %narrow_ref.1) | copy-start | bytes 6291460
  9.9 54.2 %copy-start.9 = (bf16[64,2048]{1,0:T(8,128)(2,1)S(1)}, bf16[64,2048]{1,0:T(8,128)(2,1)}, u32[]{:S(2)}) copy-start(bf16[64,2048]{1,0:T(8,128)(2,1)} %res_ref.1) | copy-start | bytes 786436
  9.9 54.2 %copy-start.10 = (f32[2048]{0:T(1024)S(1)}, f32[2048]{0:T(1024)}, u32[]{:S(2)}) copy-start(f32[2048]{0:T(1024)} %param.28) | copy-start | bytes 24580
  64.0 49.1 %copy-start.7 = (bf16[2048,256]{1,0:T(8,128)(2,1)}, bf16[2048,256]{1,0:T(8,128)(2,1)S(1)}, u32[]{:S(2)}) copy-start(bf16[2048,256]{1,0:T(8,128)(2,1)S(1)} %get-tuple-element.16.peer_gate) | copy-start | bytes 3145732
  64.1 50.1 %copy-start.6 = (bf16[1,2048,256]{2,1,0:T(8,128)(2,1)S(1)}, bf16[1,2048,256]{2,1,0:T(8,128)(2,1)}, u32[]{:S(2)}) copy-start(bf16[1,2048,256]{2,1,0:T(8,128)(2,1)} %param.31) | copy-start | bytes 3145732
  113.1 1.0 copy-start.8

commit v3 on v1

--- a/solution.py
+++ b/solution.py
@@ -12,16 +12,16 @@
 F32, BF16 = jnp.float32, jnp.bfloat16
 HW = 128
 HN = 64
-GROUPS = 4
+NX = 4
 LOG2E = math.log2(math.e)
 NEG = -1e30
 epsilon = 1e-06
 
 
 def attention_kernel(
-    dims, q_ref, kd_ref, v_ref, tot_ref, att_ref,
+    dims, q_ref, kd_ref, v_ref, tot_ref, gate_ref, up_ref, att_ref, peer_gate, peer_up,
     qb, kb, vb, tt, drow, mb, acc, ob, sb, orv, srv, ab, ar,
-    q_s, q_r, up_s, up_r, dn_s, dn_r, pr_s, pr_r, t1_s, t1_r, t2_s, t2_r, o_s, o_r, y_s, y_r, loc,
+    q_s, q_r, up_s, up_r, dn_s, dn_r, pr_s, pr_r, t1_s, t1_r, t2_s, t2_r, o_s, o_r, y_s, y_r, loc, w_s, w_r,
 ):
     nz, nx, ny = dims
     half = nz // 2
@@ -118,6 +118,14 @@
         q_copy(i).start()
     for j in range(2):
         own_pr(j).start()
+    pair = at(z, x, c, lax.rem(y, 2) * (y - 1) + (1 - lax.rem(y, 2)) * (y + 1))
+    first_rows = pl.ds(0, peer_up.shape[0])
+    weights = [
+        remote(gate_ref, peer_gate, w_s.at[0], w_r.at[0], pair),
+        remote(up_ref.at[first_rows, :], peer_up, w_s.at[1], w_r.at[1], pair),
+    ]
+    for copy in weights:
+        copy.start()
     local = [
         pltpu.make_async_copy(tot_ref, tt.at[z, xc], loc.at[0]),
         pltpu.make_async_copy(q_ref, qb.at[x], loc.at[1]),
@@ -320,6 +328,8 @@
         remote(rows_of(src), ar.at[src], y_s.at[i - 1], y_r.at[i - 1], at(z, x, c, src)).wait_recv()
         att_ref[src] = ar[src]
 
+    for copy in weights:
+        copy.wait()
     for j in range(2):
         if up_has(1, j):
             own_up(j).wait_send()
@@ -347,16 +357,21 @@
         y_copy(i).wait_send()
 
 
-def attend(dims, q, kd, v, tot):
+def attend(dims, q, kd, v, tot, gate, up):
     nz, nx, ny = dims
     half = nz // 2
     dma = pltpu.SemaphoreType.DMA
     vmem = pl.BlockSpec(memory_space=pltpu.VMEM)
+    hbm = pl.BlockSpec(memory_space=pl.ANY)
     return pl.pallas_call(
         functools.partial(attention_kernel, dims),
-        out_shape=jax.ShapeDtypeStruct((ny, 256 // ny, 256), BF16),
-        in_specs=[vmem] * 4,
-        out_specs=vmem,
+        out_shape=[
+            jax.ShapeDtypeStruct((ny, 256 // ny, 256), BF16),
+            jax.ShapeDtypeStruct(gate.shape, BF16),
+            jax.ShapeDtypeStruct((up.shape[0] // 2, up.shape[1]), BF16),
+        ],
+        in_specs=[vmem] * 4 + [hbm] * 2,
+        out_specs=[vmem, hbm, hbm],
         scratch_shapes=[
             pltpu.VMEM((nx, 256, 256), BF16),
             pltpu.VMEM((nz, 2, 272, 256), BF16),
@@ -375,12 +390,12 @@
             dma((half + 1, 2)), dma((half + 1, 2)), dma((half + 1, 2)), dma((half + 1, 2)),
             dma((nz, 2)), dma((nz, 2)),
             dma((2 * nx,)), dma((2 * nx,)), dma((nz,)), dma((nz,)),
-            dma((nx, 2)), dma((nx, 2)), dma((ny,)), dma((ny,)), dma((4,)),
+            dma((nx, 2)), dma((nx, 2)), dma((ny,)), dma((ny,)), dma((4,)), dma((2,)), dma((2,)),
         ],
         compiler_params=pltpu.CompilerParams(collective_id=1, has_side_effects=True, vmem_limit_bytes=40 * 2**20),
         cost_estimate=pl.CostEstimate(flops=10**10, bytes_accessed=10**7, transcendentals=12 * 10**6),
         name="attend",
-    )(q, kd, v, tot)
+    )(q, kd, v, tot, gate, up)
 
 
 def prepare(query_wide, key_wide, value_wide, query_narrow, key_narrow, value_narrow, gate_wide, gate_narrow):
@@ -395,6 +410,284 @@
     kd = jnp.concatenate([jnp.concatenate([key_wide, key_narrow], axis=1), parts], axis=0)
     v = jnp.concatenate([value_wide, value_narrow], axis=1)
     return q, kd, v, tot
+
+
+def paired(y):
+    return lax.rem(y, 2) * (y - 1) + (1 - lax.rem(y, 2)) * (y + 1)
+
+
+def far_first(t, nz):
+    m = nz // 2 - (t + 1) // 2
+    return jnp.where((lax.rem(t, 2) == 0) & (t > 0), -m, m)
+
+
+def moe_kernel(
+    dims, att_ref, res_ref, wide_ref, narrow_ref, gain_ref, routing_ref, weight_ref,
+    gate_ref, up_ref, down_ref, peer_gate, peer_up, out_ref,
+    ow, on, perm, tmp, snd, arr, arc, xo, xc, mid, wg, wu, wd, total, part, back, bsd, ret, rows,
+    a_s, a_r, c_s, c_r, p_s, p_r, b_s, b_r, w_s, w_r, loc,
+):
+    nz, nx, ny = dims
+    plane = 2 * nx
+    count = nz * plane
+    step = 4 * plane
+    sp, y = lax.axis_index("sp"), lax.axis_index("tp")
+    z = sp // plane
+    half = peer_up.shape[0]
+    fetch = [
+        pltpu.make_async_copy(wide_ref, ow, loc.at[0]),
+        pltpu.make_async_copy(narrow_ref, on, loc.at[1]),
+        pltpu.make_async_copy(gate_ref, wg.at[0], loc.at[2]),
+        pltpu.make_async_copy(peer_gate, wg.at[1], loc.at[3]),
+        pltpu.make_async_copy(up_ref, wu.at[0], loc.at[4]),
+        pltpu.make_async_copy(peer_up, wu.at[1, pl.ds(0, half), :], loc.at[5]),
+        pltpu.make_async_copy(down_ref, wd.at[0], loc.at[6]),
+    ]
+    for copy in fetch:
+        copy.start()
+
+    def remote(src, dst, send, recv, device):
+        return pltpu.make_async_remote_copy(
+            src_ref=src, dst_ref=dst, send_sem=send, recv_sem=recv, device_id=device, device_id_type=MESH
+        )
+
+    barrier = pltpu.get_barrier_semaphore()
+    pair, across = (sp, paired(y)), (sp, ny - 1 - y)
+
+    def greet(i, carry):
+        pl.semaphore_signal(barrier, inc=1, device_id=(lax.rem(sp + i, count), y), device_id_type=MESH)
+        return carry
+    lax.fori_loop(1, count, greet, 0)
+    pl.semaphore_signal(barrier, inc=1, device_id=pair, device_id_type=MESH)
+    pl.semaphore_signal(barrier, inc=1, device_id=across, device_id_type=MESH)
+
+    own_rows = routing_ref.shape[0]
+    names = [routing_ref[:, k:k + 1].astype(F32) for k in range(2)]
+    expert = lax.broadcasted_iota(jnp.int32, (own_rows, count), 1).astype(F32)
+    hits = [jnp.where(name == expert, 1.0, 0.0) for name in names]
+    earlier = lax.broadcasted_iota(jnp.int32, (own_rows, own_rows), 1) < lax.broadcasted_iota(
+        jnp.int32, (own_rows, own_rows), 0
+    )
+    before = jnp.dot(
+        jnp.where(earlier, 1.0, 0.0).astype(BF16), (hits[0] + hits[1]).astype(BF16), preferred_element_type=F32
+    )
+    slot = lax.broadcasted_iota(jnp.int32, (own_rows, 4 * count), 1).astype(F32)
+    chosen = [
+        slot == names[k] * 4.0 + jnp.sum(before * hits[k], axis=1, keepdims=True) for k in range(2)
+    ]
+
+    for copy in fetch[:2]:
+        copy.wait()
+    a_wide = jnp.concatenate([att_ref[k, :, :128] for k in range(ny)], axis=1)
+    a_narrow = jnp.concatenate([att_ref[k, :, 128:] for k in range(ny)], axis=1)
+    mixed = jnp.dot(a_wide, ow[...], preferred_element_type=F32) + jnp.dot(a_narrow, on[...], preferred_element_type=F32)
+    middle = (res_ref[...].astype(F32) + mixed).astype(BF16)
+    mid[...] = middle
+    middle = middle.astype(F32)
+    spread = jnp.mean(middle * middle, axis=1, keepdims=True)
+    normed = (middle * lax.rsqrt(spread + epsilon) * gain_ref[...]).astype(BF16)
+    picker = jnp.where(chosen[0] | chosen[1], 1.0, 0.0).astype(BF16)
+    perm[...] = lax.dot_general(picker, normed, (((0,), (0,)), ((), ())), preferred_element_type=F32)
+
+    def cut(k, carry):
+        v = perm[pl.ds(pl.multiple_of(8 * k, 8), 8), :]
+        snd[2 * k] = v[:4].astype(BF16)
+        snd[2 * k + 1] = v[4:].astype(BF16)
+        return carry
+    lax.fori_loop(0, count // 2, cut, 0)
+    pl.semaphore_wait(barrier, count - 1 + 2)
+
+    def to_plane(t):
+        return lax.rem(z + far_first(t, nz) + nz, nz)
+
+    def from_plane(t):
+        return lax.rem(z - far_first(t, nz) + nz, nz)
+
+    def out_copy(e):
+        return remote(snd.at[e], arr.at[sp], a_s.at[e], a_r.at[sp], (e, y))
+
+    def each_other(p, act):
+        def one(k, carry):
+            e = p * plane + k
+
+            @pl.when(e != sp)
+            def _():
+                act(e)
+            return carry
+        lax.fori_loop(0, plane, one, 0)
+
+    def send(t, carry):
+        each_other(to_plane(t), lambda e: out_copy(e).start())
+        return carry
+    lax.fori_loop(0, nz, send, 0)
+    weights = [
+        remote(up_ref.at[pl.ds(half, half), :], wu.at[1, pl.ds(half, half), :], w_s.at[0], w_r.at[0], pair),
+        remote(down_ref, wd.at[1], w_s.at[1], w_r.at[1], pair),
+    ]
+    for copy in weights:
+        copy.start()
+    keep = pltpu.make_async_copy(snd.at[sp], arr.at[sp], loc.at[7])
+    keep.start()
+    keep.wait()
+
+    def to_rows(take):
+        for k in range(plane // 2):
+            tmp[8 * k:8 * k + 8, :] = jnp.concatenate([take(2 * k).astype(F32), take(2 * k + 1).astype(F32)], axis=0)
+
+    def rows_at(t):
+        return pl.ds(pl.multiple_of(t * step, step), step)
+
+    def cross_copy(p):
+        some = pl.ds(p * plane, plane)
+        return remote(arr.at[some], arc.at[some], c_s.at[p], c_r.at[p], across)
+
+    def arrive_cross(t):
+        p = from_plane(t)
+        cross_copy(p).wait_recv()
+        to_rows(lambda k: arc[p * plane + k])
+        xc[rows_at(t), :] = tmp[...].astype(BF16)
+
+    def arrive(t, carry):
+        p = from_plane(t)
+        each_other(p, lambda s: remote(snd.at[s], arr.at[s], a_s.at[s], a_r.at[s], (s, y)).wait_recv())
+        cross_copy(p).start()
+        to_rows(lambda k: arr[p * plane + k])
+        xo[rows_at(t), :] = tmp[...].astype(BF16)
+
+        @pl.when(t >= nz // 2)
+        def _():
+            arrive_cross(t - nz // 2)
+        return carry
+    lax.fori_loop(0, nz, arrive, 0)
+    for copy in fetch[2:]:
+        copy.wait()
+    for copy in weights:
+        copy.wait_recv()
+
+    def hidden(x):
+        both = []
+        for k in range(2):
+            g = jnp.dot(x, wg[k], preferred_element_type=F32)
+            u = jnp.dot(x, wu[k], preferred_element_type=F32)
+            both.append((jax.nn.silu(g) * u).astype(BF16))
+        return both
+
+    def down(h, put):
+        width = 512
+        for q in range(wd.shape[2] // width):
+            cols = slice(q * width, (q + 1) * width)
+            put(
+                cols,
+                jnp.dot(h[0], wd[0, :, cols], preferred_element_type=F32)
+                + jnp.dot(h[1], wd[1, :, cols], preferred_element_type=F32),
+            )
+
+    def part_copy(t):
+        some = rows_at(t)
+        return remote(part.at[some, :], back.at[some, :], p_s.at[t], p_r.at[t], across)
+
+    def send_part(t, carry):
+        part_copy(t).start()
+        return carry
+
+    def cross_half(k):
+        some = slice(k * step * nz // 2, (k + 1) * step * nz // 2)
+
+        def put(cols, value):
+            part[some, cols] = value.astype(BF16)
+        down(hidden(xc[some, :]), put)
+        lax.fori_loop(k * nz // 2, (k + 1) * nz // 2, send_part, 0)
+
+    cross_half(0)
+
+    def put_total(cols, value):
+        total[:, cols] = value
+    down(hidden(xo[...]), put_total)
+
+    def late(t, carry):
+        arrive_cross(t)
+        return carry
+    lax.fori_loop(nz // 2, nz, late, 0)
+    cross_half(1)
+
+    def back_copy(e):
+        return remote(bsd.at[e], ret.at[sp], b_s.at[e], b_r.at[sp], (e, y))
+
+    def finish(t, carry):
+        p = from_plane(t)
+        part_copy(t).wait_recv()
+        some = rows_at(t)
+        tmp[...] = total[some, :] + back[some, :].astype(F32)
+        for k in range(plane // 2):
+            v = tmp[8 * k:8 * k + 8, :]
+            bsd[p * plane + 2 * k] = v[:4].astype(BF16)
+            bsd[p * plane + 2 * k + 1] = v[4:].astype(BF16)
+        each_other(p, lambda e: back_copy(e).start())
+        return carry
+    lax.fori_loop(0, nz, finish, 0)
+    last = pltpu.make_async_copy(bsd.at[sp], ret.at[sp], loc.at[8])
+    last.start()
+    last.wait()
+
+    def returned(t, carry):
+        p = to_plane(t)
+        each_other(p, lambda e: remote(bsd.at[e], ret.at[e], b_s.at[e], b_r.at[e], (e, y)).wait_recv())
+        to_rows(lambda k: ret[p * plane + k])
+        rows[rows_at(p), :] = tmp[...].astype(BF16)
+        return carry
+    lax.fori_loop(0, nz, returned, 0)
+    share = jnp.where(chosen[0], weight_ref[:, 0:1], 0.0) + jnp.where(chosen[1], weight_ref[:, 1:2], 0.0)
+    combined = mid[...].astype(F32)
+    for _ in range(3):
+        term = share.astype(BF16)
+        share = share - term.astype(F32)
+        combined = combined + jnp.dot(term, rows[...], preferred_element_type=F32)
+    out_ref[...] = combined.astype(BF16)
+
+    for copy in weights:
+        copy.wait_send()
+
+    def drain(t, carry):
+        each_other(t, lambda e: out_copy(e).wait_send())
+        each_other(t, lambda e: back_copy(e).wait_send())
+        cross_copy(t).wait_send()
+        part_copy(t).wait_send()
+        return carry
+    lax.fori_loop(0, nz, drain, 0)
+
+
+def experts(dims, att, residual, wide, narrow, gain, routing, route_weight, gate, up, down, peer_gate, peer_up):
+    nz, nx, ny = dims
+    count, features = nz * nx * 2, residual.shape[1]
+    dma = pltpu.SemaphoreType.DMA
+    vmem = pl.BlockSpec(memory_space=pltpu.VMEM)
+    hbm = pl.BlockSpec(memory_space=pl.ANY)
+    blocks = pltpu.VMEM((count, 4, features), BF16)
+    table = pltpu.VMEM((4 * count, features), BF16)
+    return pl.pallas_call(
+        functools.partial(moe_kernel, dims),
+        out_shape=jax.ShapeDtypeStruct(residual.shape, BF16),
+        in_specs=[vmem, vmem, hbm, hbm, vmem, vmem, vmem] + [hbm] * 5,
+        out_specs=vmem,
+        scratch_shapes=[
+            pltpu.VMEM(wide.shape, BF16),
+            pltpu.VMEM(narrow.shape, BF16),
+            pltpu.VMEM((4 * count, features), F32),
+            pltpu.VMEM((8 * nx, features), F32),
+            blocks, blocks, blocks, table, table,
+            pltpu.VMEM(residual.shape, BF16),
+            pltpu.VMEM((2, *gate.shape), BF16),
+            pltpu.VMEM((2, *up.shape), BF16),
+            pltpu.VMEM((2, *down.shape), BF16),
+            pltpu.VMEM((4 * count, features), F32),
+            table, table, blocks, blocks, table,
+            dma((count,)), dma((count,)), dma((nz,)), dma((nz,)), dma((nz,)), dma((nz,)),
+            dma((count,)), dma((count,)), dma((2,)), dma((2,)), dma((9,)),
+        ],
+        compiler_params=pltpu.CompilerParams(collective_id=2, has_side_effects=True, vmem_limit_bytes=48 * 2**20),
+        cost_estimate=pl.CostEstimate(flops=10**9, bytes_accessed=10**7, transcendentals=1000),
+        name="experts",
+    )(att, residual, wide, narrow, gain, routing, route_weight, gate, up, down, peer_gate, peer_up)
 
 
 def body(
@@ -417,62 +710,17 @@
     down_weight,
 ):
     ny = lax.axis_size("tp")
-    nx = 4
+    nx = NX
     dims = (lax.axis_size("sp") // (2 * nx), nx, ny)
-    own_rows = residual.shape[0]
-    full_gate = lax.all_gather(gate_weight[0], "tp", axis=0)
-    full_up = lax.all_gather(up_weight[0], "tp", axis=0)
-    full_down = lax.all_gather(down_weight[0], "tp", axis=0, tiled=True)
-    att = attend(
-        dims,
-        *prepare(
-            query_wide, key_wide, value_wide, query_narrow, key_narrow, value_narrow, gate_wide, gate_narrow
-        ),
+    gate, up, down = gate_weight[0], up_weight[0], down_weight[0]
+    ready = prepare(
+        query_wide, key_wide, value_wide, query_narrow, key_narrow, value_narrow, gate_wide, gate_narrow
     )
-    heads_wide = jnp.transpose(att[:, :, :128], (1, 0, 2)).reshape(own_rows, 128 * ny)
-    heads_narrow = jnp.transpose(att[:, :, 128:], (1, 0, 2)).reshape(own_rows, 128 * ny)
-    mixed = jnp.dot(heads_wide, out_wide, preferred_element_type=jnp.float32)
-    mixed = mixed + jnp.dot(heads_narrow, out_narrow, preferred_element_type=jnp.float32)
-    middle = (residual.astype(jnp.float32) + mixed).astype(jnp.bfloat16)
-    middle_wide = middle.astype(jnp.float32)
-    spread = jnp.mean(middle_wide * middle_wide, axis=1, keepdims=True)
-    normed = (middle_wide * lax.rsqrt(spread + epsilon) * norm_gain).astype(jnp.bfloat16)
-    features = normed.shape[1]
-    chosen_count = routing.shape[1]
-    expert_count = gate_weight.shape[0] * lax.axis_size("sp")
-    capacity = own_rows * GROUPS // expert_count
-    flat_routes = routing.reshape(-1)
-    matches = (flat_routes[:, None] == jnp.arange(expert_count, dtype=jnp.int32)[None, :]).astype(
-        jnp.int32
+    att, peer_gate, peer_up = attend(dims, *ready, gate, up)
+    return experts(
+        dims, att, residual, out_wide, out_narrow, norm_gain[None, :], routing, route_weight,
+        gate, up, down, peer_gate, peer_up,
     )
-    ranking = jnp.sum((jnp.cumsum(matches, axis=0) - matches) * matches, axis=1)
-    placing = flat_routes * capacity + ranking
-    picker = (
-        placing[None, :] == jnp.arange(expert_count * capacity, dtype=jnp.int32)[:, None]
-    ).astype(jnp.bfloat16)
-    picker = jnp.sum(picker.reshape(expert_count * capacity, own_rows, chosen_count), axis=2)
-    outgoing = jnp.dot(picker, normed, preferred_element_type=jnp.float32).astype(jnp.bfloat16)
-    outgoing = outgoing.reshape(expert_count, capacity, features)
-    arrived = lax.all_to_all(outgoing, "sp", split_axis=0, concat_axis=0, tiled=True)
-    rows = arrived.reshape(-1, features)
-    hidden = []
-    for k in range(ny):
-        gate_value = jnp.dot(rows, full_gate[k], preferred_element_type=jnp.float32)
-        up_value = jnp.dot(rows, full_up[k], preferred_element_type=jnp.float32)
-        hidden.append((jax.nn.silu(gate_value) * up_value).astype(jnp.bfloat16))
-    hidden = jnp.concatenate(hidden, axis=1)
-    answers = jnp.dot(hidden, full_down, preferred_element_type=jnp.float32).astype(jnp.bfloat16)
-    returned = lax.all_to_all(
-        answers.reshape(expert_count, capacity, features),
-        "sp",
-        split_axis=0,
-        concat_axis=0,
-        tiled=True,
-    )
-    picked = jnp.take(returned.reshape(expert_count * capacity, features), placing, axis=0)
-    picked = picked.reshape(own_rows, chosen_count, features).astype(jnp.float32)
-    combined = jnp.sum(route_weight[:, :, None] * picked, axis=1)
-    return (middle_wide + combined).astype(jnp.bfloat16)
 
 
 def solution(mesh):

time: 231 us -> 155 us (0.67)
  Pallas kernels: 54.1 us -> 140 us
  waiting for transfers between devices: 66 us -> 0 us
  blocking collectives: 43.1 us -> 0 us
  matrix products: 22.5 us -> 0 us
  between operations: 13.4 us -> 0.14 us
  starting transfers between devices: 11.1 us -> 0 us
  other arithmetic: 9.23 us -> 3.64 us
    pallas_call x1 -> x2, Pallas kernels: 54.1 us -> 140 us  [the longest x1 85.9 us: experts(): pl.pallas_call(functools.partial(moe_kernel, dims), out_shape=jax.ShapeDt...]
    all_to_all x1 -> x0, blocking collectives: 43.1 us -> none  [body(): lax.all_to_all(outgoing, 'sp', split_axis=0, concat_axis=0, tiled=True)]
    all_gather x3 -> x0, waiting for transfers between devices: 36.3 us -> none  [the longest x1 36.3 us: body(): full_down = lax.all_gather(down_weight[0], 'tp', axis=0, tiled=True)]
    all_to_all x1 -> x0, waiting for transfers between devices: 27.6 us -> none  [body(): lax.all_to_all(answers.reshape(expert_count, capacity, features), 'sp', s...]
    dot_general x12 -> x0, matrix products: 22.5 us -> none  [the longest x4 9.8 us: body(): gate_value = jnp.dot(rows, full_gate[k], preferred_element_type=jnp.float32)]
    all_to_all x1 -> x0, starting transfers between devices: 11 us -> none  [body(): lax.all_to_all(answers.reshape(expert_count, capacity, features), 'sp', s...]
    unnamed x23 -> x29, local copies, waits for them, and re-layouts: 1.71 us -> 10.3 us
    reshape x6 -> x1, local copies, waits for them, and re-layouts: 5.11 us -> 0.01 us  [the longest x1 1.33 us: body(): returned.reshape(expert_count * capacity, features)]
  transfers between devices with their start and end apart: 4 -> 0, of which waited for: 2 -> 0; matrix products, arithmetic and copies ran while one was open for 12% -> 0% of each run, Pallas kernels for 23% -> 0%
where the time goes in v3:
time: 155 us
  Pallas kernels  140 us (90%)
  local copies, waits for them, and re-layouts  10.8 us (7%)
  other arithmetic  3.64 us (2%)
    pallas_call x1, Pallas kernels, experts(): pl.pallas_call(functools.partial(moe_kernel, dims), out_shape=jax.ShapeDt...  85.9 us
    pallas_call x1, Pallas kernels, attend(): pl.pallas_call(functools.partial(attention_kernel, dims), out_shape=[jax....  54.1 us
    unnamed x29, local copies, waits for them, and re-layouts  10.3 us

profile of v3, /device:TPU:1, one launch (start us, length us, event | category | flops | bytes accessed | tf_op | source)
XLA Modules:
  0.0 154.7 jit_solution(38972449613959766)
XLA Ops:
  0.0 0.7 fusion.4
  0.7 0.9 reduce-window.6
  1.7 0.1 slice.12
  1.7 0.1 copy.25
  1.9 0.1 copy.26
  2.0 0.1 add_multiply_fusion
  2.1 0.9 fusion.1.kd_ref
  3.0 0.1 copy.31
  3.2 1.0 pad_maximum_fusion
  4.2 0.0 copy-start
  4.2 1.2 copy-done
  5.4 0.0 copy-start.2
  5.4 1.2 copy-done.2
  6.6 0.0 copy-start.1
  6.6 0.0 copy-start.3
  6.6 0.0 copy-start.4
  6.6 0.0 copy-start.9
  6.6 0.0 copy-start.12
  6.6 54.1 %attend.1 = (bf16[4,64,256]{2,1,0:T(8,128)(2,1)S(1)}, bf16[2048,256]{1,0:T(8,128)(2,1)S(1)}, bf16[1024,256]{1,0:T(8,128)(2,1)S(1)}) custom-call(bf16[256,256]{1,0:T(8,128)(2,1)S(1)} %get-tuple-element.14.q_ref, bf16[272,256]{1,0:T(8,128)(2,1)S(1)} %fusion.1.kd_ref, bf16[256,256]{1,0:T(8,128)(2,1)S(1)} %get-tuple-element.15.v_ref, ...), custom_call_target="tpu_custom_call" | custom-call | flops 10000000000 | bytes 10000000 | tf_op jit(solution)/shard_map/attend/pallas_call | solution.py:366
  60.8 0.0 copy-start.5
  60.8 1.0 copy-done.5
  61.8 0.0 copy-start.7
  61.8 0.8 copy-done.7
  62.6 0.0 copy-start.10
  62.6 0.7 copy-done.10
  63.2 0.8 copy.29.routing_ref
  64.0 0.8 copy.30.weight_ref
  64.8 0.0 copy-done.1
  64.8 0.0 copy-done.3
  64.8 0.0 copy-done.4
  64.8 0.0 copy-done.9
  64.8 0.0 copy-done.12
  64.8 0.0 copy-start.6
  64.8 1.2 copy-done.6
  66.0 0.0 copy-start.8
  66.0 1.0 copy-done.8
  67.1 0.0 copy-start.11
  67.1 0.9 copy-done.11
  68.0 85.9 %experts.1 = bf16[64,2048]{1,0:T(8,128)(2,1)S(1)} custom-call(bf16[4,64,256]{2,1,0:T(8,128)(2,1)S(1)} %copy-done.11, bf16[64,2048]{1,0:T(8,128)(2,1)S(1)} %copy-done.9, bf16[512,2048]{1,0:T(8,128)(2,1)} %wide_ref.1, bf16[512,2048]{1,0:T(8,128)(2,1)} %narrow_ref.1, f32[1,2048]{1,0:T(1,128)S(1)} %bitcast.17, s32[64,2]{1,0:T(8,128)S(1)} %copy.29.routing_ref, ...), custom_call_target="tpu_custom_call" | custom-call | flops 1000000000 | bytes 10000000 | tf_op jit(solution)/shard_map/experts/pallas_call | solution.py:667
  153.9 0.7 copy.33
  (10 shorter events, 0.1 us)
Async XLA Ops:
  4.2 1.2 copy-start
  5.4 1.2 copy-start.2
  6.6 58.2 %copy-start.1 = (bf16[1,2048,256]{2,1,0:T(8,128)(2,1)S(1)}, bf16[1,2048,256]{2,1,0:T(8,128)(2,1)}, u32[]{:S(2)}) copy-start(bf16[1,2048,256]{2,1,0:T(8,128)(2,1)} %param.31) | copy-start | bytes 3145732
  6.6 58.2 %copy-start.3 = (bf16[1,2048,256]{2,1,0:T(8,128)(2,1)S(1)}, bf16[1,2048,256]{2,1,0:T(8,128)(2,1)}, u32[]{:S(2)}) copy-start(bf16[1,2048,256]{2,1,0:T(8,128)(2,1)} %param.32) | copy-start | bytes 3145732
  6.6 58.2 %copy-start.4 = (bf16[1,256,2048]{2,1,0:T(8,128)(2,1)S(1)}, bf16[1,256,2048]{2,1,0:T(8,128)(2,1)}, u32[]{:S(2)}) copy-start(bf16[1,256,2048]{2,1,0:T(8,128)(2,1)} %param.33) | copy-start | bytes 3145732
  6.6 58.2 %copy-start.9 = (bf16[64,2048]{1,0:T(8,128)(2,1)S(1)}, bf16[64,2048]{1,0:T(8,128)(2,1)}, u32[]{:S(2)}) copy-start(bf16[64,2048]{1,0:T(8,128)(2,1)} %res_ref.1) | copy-start | bytes 786436
  6.6 58.2 %copy-start.12 = (f32[2048]{0:T(1024)S(1)}, f32[2048]{0:T(1024)}, u32[]{:S(2)}) copy-start(f32[2048]{0:T(1024)} %param.28) | copy-start | bytes 24580
  60.8 1.0 copy-start.5
  61.8 0.8 copy-start.7
  62.6 0.7 copy-start.10
  64.8 1.2 copy-start.6
  66.0 1.0 copy-start.8
  67.1 0.9 copy-start.11

commit v4 on v3

v4 whole, which is shorter than its diff:
```python
import functools
import math

import jax
import jax.numpy as jnp
from jax import lax
from jax.experimental import pallas as pl
from jax.experimental.pallas import tpu as pltpu
from jax.sharding import PartitionSpec as P

MESH = pl.DeviceIdType.MESH
F32, BF16 = jnp.float32, jnp.bfloat16
HW = 128
HN = 64
NX = 4
LOG2E = math.log2(math.e)
NEG = -1e30
LOWEST = -1e20
epsilon = 1e-06


def paired(y):
    return lax.rem(y, 2) * (y - 1) + (1 - lax.rem(y, 2)) * (y + 1)


def far_first(t, nz):
    m = nz // 2 - (t + 1) // 2
    return jnp.where((lax.rem(t, 2) == 0) & (t > 0), -m, m)


def layer_kernel(
    dims, res_ref, qw_ref, kw_ref, vw_ref, qn_ref, kn_ref, vn_ref, gw_ref, gn_ref, wide_ref, narrow_ref, gain_ref,
    routing_ref, weight_ref, gate_ref, up_ref, down_ref, out_ref,
    q_ref, kd_ref, v_ref, tot_ref, qb, kb, vb, tt, kaug, mb, acc, ob, sb, orv, srv, ab, ar,
    q_s, q_r, up_s, up_r, dn_s, dn_r, pr_s, pr_r, t1_s, t1_r, t2_s, t2_r, o_s, o_r, y_s, y_r, loc,
    ow, on, perm, tmp, snd, arr, arc, xo, xs, mid, wg, wu, wd, total, part, back, bsd, ret, rows,
    a_s, a_r, c_s, c_r, p_s, p_r, b_s, b_r, w_s, w_r, loc2,
):
    nz, nx, ny = dims
    half = nz // 2
    plane = 2 * nx
    count = nz * plane
    step = 4 * plane
    sp, y = lax.axis_index("sp"), lax.axis_index("tp")
    fetch = [
        pltpu.make_async_copy(wide_ref, ow, loc2.at[0]),
        pltpu.make_async_copy(narrow_ref, on, loc2.at[1]),
        pltpu.make_async_copy(gate_ref, wg.at[0], loc2.at[2]),
        pltpu.make_async_copy(up_ref, wu.at[0], loc2.at[3]),
        pltpu.make_async_copy(down_ref, wd.at[0], loc2.at[4]),
    ]
    for copy in fetch:
        copy.start()
    c = lax.rem(sp, 2)
    x = lax.rem(sp // 2, nx)
    z = sp // (2 * nx)
    xc = x * 2 + c

    def at(z_, x_, c_, y_):
        return ((z_ * nx + x_) * 2 + c_, y_)

    def zup(i):
        return lax.rem(z + i, nz)

    def zdn(i):
        return lax.rem(z - i + nz, nz)

    def in_plane(i):
        other = lax.rem(xc + i, 2 * nx)
        return at(z, other // 2, lax.rem(other, 2), y)

    def remote(src, dst, send, recv, device):
        return pltpu.make_async_remote_copy(
            src_ref=src, dst_ref=dst, send_sem=send, recv_sem=recv, device_id=device, device_id_type=MESH
        )

    barrier = pltpu.get_barrier_semaphore()

    def greet(device):
        pl.semaphore_signal(barrier, inc=1, device_id=device, device_id_type=MESH)

    def greet_along(i, carry):
        greet((lax.rem(sp + i, count), y))
        return carry
    lax.fori_loop(1, count, greet_along, 0)
    for i in range(1, ny):
        greet((sp, lax.rem(y + i, ny)))
    lane = lax.broadcasted_iota(jnp.int32, (1, 128), 1)
    gates = jnp.where(lane == 0, gw_ref[...], jnp.where(lane == 1, gn_ref[:, 0:1], gn_ref[:, 1:2]))
    logs = jnp.minimum(gates, 0.0) - jnp.log1p(jnp.exp(-jnp.abs(gates)))
    logs = jnp.where(lane < 3, logs, 0.0)
    until = lax.broadcasted_iota(jnp.int32, (256, 256), 1) <= lax.broadcasted_iota(jnp.int32, (256, 256), 0)
    until = jnp.where(until, 1.0, 0.0).astype(BF16)
    run = jnp.zeros((256, 128), F32)
    for _ in range(3):
        term = logs.astype(BF16)
        logs = logs - term.astype(F32)
        run = run + jnp.dot(until, term, preferred_element_type=F32)
    run = run * LOG2E
    tot_ref[...] = run[255:256]
    left = jnp.transpose(run)[:8]
    terms = []
    for _ in range(3):
        term = left.astype(BF16).astype(F32)
        left = left - term
        terms.append(term)
    kd_ref[256:288, :] = jnp.concatenate(terms + [jnp.zeros((8, 256), F32)], axis=0).astype(BF16)
    kd_ref[0:256, :128] = kw_ref[...]
    kd_ref[0:256, 128:] = kn_ref[...]
    v_ref[0:128, :] = jnp.transpose(vw_ref[...].astype(F32)).astype(BF16)
    v_ref[128:256, :] = jnp.transpose(vn_ref[...].astype(F32)).astype(BF16)
    q_ref[0:128, :] = jnp.transpose(qw_ref[...].astype(F32) * (HW ** -0.5 * LOG2E)).astype(BF16)
    q_ref[128:256, :] = jnp.transpose(qn_ref[...].astype(F32) * (HN ** -0.5 * LOG2E)).astype(BF16)
    own_rows = routing_ref.shape[0]
    names = [routing_ref[:, k:k + 1].astype(F32) for k in range(2)]
    expert = lax.broadcasted_iota(jnp.int32, (own_rows, count), 1).astype(F32)
    hits = [jnp.where(name == expert, 1.0, 0.0) for name in names]
    earlier = lax.broadcasted_iota(jnp.int32, (own_rows, own_rows), 1) < lax.broadcasted_iota(
        jnp.int32, (own_rows, own_rows), 0
    )
    before = jnp.dot(
        jnp.where(earlier, 1.0, 0.0).astype(BF16), (hits[0] + hits[1]).astype(BF16), preferred_element_type=F32
    )
    slot = lax.broadcasted_iota(jnp.int32, (own_rows, 4 * count), 1).astype(F32)
    chosen = [
        slot == names[k] * 4.0 + jnp.sum(before * hits[k], axis=1, keepdims=True) for k in range(2)
    ]
    pl.semaphore_wait(barrier, count - 1 + ny - 1)

    up_dev, dn_dev, pr_dev = at(zup(1), x, c, y), at(zdn(1), x, c, y), at(z, x, 1 - c, y)

    def up_copy(s, j):
        zb = zdn(s)
        src = (kb, vb)[j].at[zb, c]
        return remote(src, src, up_s.at[s, j], up_r.at[s, j], up_dev)

    def dn_copy(s, j):
        zb = zup(s)
        src = (kb, vb)[j].at[zb, c]
        return remote(src, src, dn_s.at[s, j], dn_r.at[s, j], dn_dev)

    def pr_copy(zb, j):
        src = (kb, vb)[j].at[zb, c]
        return remote(src, src, pr_s.at[zb, j], pr_r.at[zb, j], pr_dev)

    def pr_wait(zb, j):
        dst = (kb, vb)[j].at[zb, 1 - c]
        remote(dst, dst, pr_s.at[zb, j], pr_r.at[zb, j], pr_dev).wait_recv()

    def own_up(j):
        return remote((kd_ref, v_ref)[j], (kb, vb)[j].at[z, c], up_s.at[0, j], up_r.at[0, j], up_dev)

    def own_dn(j):
        return remote((kd_ref, v_ref)[j], (kb, vb)[j].at[z, c], dn_s.at[0, j], dn_r.at[0, j], dn_dev)

    def own_pr(j):
        return remote((kd_ref, v_ref)[j], (kb, vb)[j].at[z, c], pr_s.at[z, j], pr_r.at[z, j], pr_dev)

    def up_has(s, j):
        return s < half or (s == half and j == 0)

    def dn_has(s, j):
        return s < half or (s == half and j == 1)

    for j in range(2):
        if up_has(1, j):
            own_up(j).start()
        if dn_has(1, j):
            own_dn(j).start()

    def t1_copy(i):
        return remote(tot_ref, tt.at[z, xc], t1_s.at[i - 1], t1_r.at[i - 1], in_plane(i))

    def t2_copy(i):
        return remote(tt.at[z], tt.at[z], t2_s.at[i - 1], t2_r.at[i - 1], at(zup(i), x, c, y))

    def q_copy(i):
        return remote(q_ref, qb.at[x], q_s.at[i - 1], q_r.at[i - 1], at(z, lax.rem(x + i, nx), c, y))

    for i in range(1, 2 * nx):
        t1_copy(i).start()
    for i in range(1, nx):
        q_copy(i).start()
    for j in range(2):
        own_pr(j).start()
    pair, across = (sp, paired(y)), (sp, ny - 1 - y)
    cut_at = up_ref.shape[0] * 3 // 4
    early, rest = pl.ds(0, cut_at), pl.ds(cut_at, up_ref.shape[0] - cut_at)
    weights = [
        remote(gate_ref, wg.at[1], w_s.at[0], w_r.at[0], pair),
        remote(up_ref.at[early, :], wu.at[1, early, :], w_s.at[1], w_r.at[1], pair),
        remote(up_ref.at[rest, :], wu.at[1, rest, :], w_s.at[2], w_r.at[2], pair),
        remote(down_ref, wd.at[1], w_s.at[3], w_r.at[3], pair),
    ]
    for copy in weights[:2]:
        copy.start()
    local = [
        pltpu.make_async_copy(tot_ref, tt.at[z, xc], loc.at[0]),
        pltpu.make_async_copy(q_ref, qb.at[x], loc.at[1]),
        pltpu.make_async_copy(kd_ref, kb.at[z, c], loc.at[2]),
        pltpu.make_async_copy(v_ref, vb.at[z, c], loc.at[3]),
    ]
    for copy in local:
        copy.start()
    mb[...] = jnp.full(mb.shape, LOWEST, F32)
    acc[...] = jnp.zeros(acc.shape, F32)
    local[0].wait()
    for i in range(1, 2 * nx):
        other = lax.rem(xc - i + 2 * nx, 2 * nx)
        remote(tot_ref, tt.at[z, other], t1_s.at[i - 1], t1_r.at[i - 1], in_plane(i)).wait_recv()
    for i in range(1, nz):
        t2_copy(i).start()
    for copy in local[1:]:
        copy.wait()

    def relay(s):
        for j in range(2):
            @pl.when(s <= (half if j == 0 else half - 1))
            def _():
                slot = (kb, vb)[j].at[zdn(s), c]
                remote(slot, slot, up_s.at[s - 1, j], up_r.at[s - 1, j], up_dev).wait_recv()

                @pl.when(s + 1 <= (half if j == 0 else half - 1))
                def _():
                    up_copy(s, j).start()
                pr_copy(zdn(s), j).start()

            @pl.when(s <= (half if j == 1 else half - 1))
            def _():
                slot = (kb, vb)[j].at[zup(s), c]
                remote(slot, slot, dn_s.at[s - 1, j], dn_r.at[s - 1, j], dn_dev).wait_recv()

                @pl.when(s + 1 <= (half if j == 1 else half - 1))
                def _():
                    dn_copy(s, j).start()
                pr_copy(zup(s), j).start()

    low = lax.broadcasted_iota(jnp.int32, (128, 1), 0) < HN

    def head_offsets(zb):
        def plane(p, run):
            whole = jnp.zeros((1, 128), F32)
            for k in range(2 * nx):
                whole = whole + tt[p, k]
            return run + jnp.where(p < zb, whole, 0.0)
        run = lax.fori_loop(0, nz, plane, jnp.zeros((1, 128), F32))
        for k in range(2 * nx):
            run = run + jnp.where(k < 2 * x, tt[zb, k], 0.0)
        return run, run + tt[zb, 2 * x]

    def offsets(zb):
        return [
            [jnp.sum(jnp.where(lane == h, row, 0.0), axis=1, keepdims=True) for h in range(3)]
            for row in head_offsets(zb)
        ]

    def make_kaug(zb):
        for k in range(2):
            part = jnp.concatenate([kb[zb, k, 256:288, :].astype(F32), jnp.zeros((96, 256), F32)], axis=0)
            kaug[256 * k:256 * k + 256, :] = jnp.transpose(part).astype(BF16)

    spans = ((0, 128), (144, 64), (224, 64))
    row_of = lax.broadcasted_iota(jnp.int32, (128, 256), 0)
    minus = [jnp.where((lax.rem(row_of, 8) == h) & (row_of < 24), -1.0, 0.0).astype(BF16) for h in range(3)]

    def tiles(zb, offs, masked):
        keys = jnp.concatenate([kb[zb, 0, 0:256, :], kb[zb, 1, 0:256, :]], axis=0)
        vals = jnp.concatenate([vb[zb, 0], vb[zb, 1]], axis=1)
        more = kaug[...]
        ones = jnp.ones((16, 512), BF16)
        work = [(xq, h) for xq in range(nx) for h in range(3)]
        scores, weights_, shrinks = [], [], []
        for xq, h in work:
            side = slice(0, 128) if h == 0 else slice(128, 256)
            q = qb[xq, side, :]
            if h > 0:
                q = jnp.where(low if h == 1 else jnp.logical_not(low), q, jnp.zeros_like(q))
            scores.append(
                jnp.dot(
                    jnp.concatenate([keys[:, side], more], axis=1),
                    jnp.concatenate([q, minus[h]], axis=0),
                    preferred_element_type=F32,
                )
            )
        for (xq, h), r in zip(work, scores):
            if masked:
                places = lax.broadcasted_iota(jnp.int32, (512, 256), 0) + x * 512
                wanted = lax.broadcasted_iota(jnp.int32, (512, 256), 1) + (xq * 512 + c * 256)
                r = jnp.where(places <= wanted, r, NEG)
            old = mb[xq, h]
            new = old
            for k in range(2):
                new = jnp.maximum(new, jnp.max(r[256 * k:256 * k + 256], axis=0, keepdims=True) - offs[k][h])
            weights_.append(
                jnp.concatenate(
                    [jnp.exp2(r[256 * k:256 * k + 256] - (new + offs[k][h])).astype(BF16) for k in range(2)], axis=0
                )
            )
            shrinks.append(jnp.exp2(old - new))
            mb[xq, h] = new
        for (xq, h), p, shrink in zip(work, weights_, shrinks):
            first, size = ((0, 128), (128, 64), (192, 64))[h]
            pv = jnp.dot(jnp.concatenate([vals[first:first + size], ones], axis=0), p, preferred_element_type=F32)
            some = slice(spans[h][0], spans[h][0] + size + 16)
            acc[xq, some, :] = acc[xq, some, :] * shrink + pv

    def both(zb):
        make_kaug(zb)
        tiles(zb, offsets(zb), False)

    relay(jnp.int32(1))
    for i in range(1, nx):
        src = lax.rem(x - i + nx, nx)
        remote(q_ref, qb.at[src], q_s.at[i - 1], q_r.at[i - 1], at(z, src, c, y)).wait_recv()
    for i in range(1, nz):
        slot = tt.at[zdn(i)]
        remote(slot, slot, t2_s.at[i - 1], t2_r.at[i - 1], at(zdn(i), x, c, y)).wait_recv()
    for j in range(2):
        pr_wait(z, j)
    make_kaug(z)
    tiles(z, offsets(z), True)

    def one_step(s, carry):
        @pl.when(s < half)
        def _():
            relay(s + 1)
        for j in range(2):
            pr_wait(zdn(s), j)

            @pl.when(s < half)
            def _():
                pr_wait(zup(s), j)

        def side(w, inner):
            zb = jnp.where(w == 0, zdn(s), zup(s))

            @pl.when(((w == 0) & (z >= s)) | ((w == 1) & (z + s >= nz) & (s < half)))
            def _():
                both(zb)
            return inner
        return lax.fori_loop(0, 2, side, carry)
    lax.fori_loop(1, half + 1, one_step, 0)

    def o_copies(i):
        dev = at(z, lax.rem(x + i, nx), c, y)
        return (
            remote(ob.at[i], orv.at[i], o_s.at[i, 0], o_r.at[i, 0], dev),
            remote(sb.at[i], srv.at[i], o_s.at[i, 1], o_r.at[i, 1], dev),
        )

    def last(k, carry):
        i = lax.rem(k + 1, nx)
        xq = lax.rem(x + i, nx)

        outs, lses = [], []
        for h in range(3):
            first, size = spans[h]
            total = acc[xq, pl.ds(first + size, 1), :]
            some = total > 0.0
            safe = jnp.where(some, total, 1.0)
            outs.append(acc[xq, pl.ds(first, size), :] / safe)
            lses.append(jnp.where(some, mb[xq, h] + jnp.log2(safe), NEG))
        ob[i] = jnp.concatenate(outs, axis=0).astype(BF16)
        place = lax.broadcasted_iota(jnp.int32, (8, 256), 0)
        sb[i] = jnp.where(place == 0, lses[0], jnp.where(place == 1, lses[1], lses[2]))

        @pl.when(i > 0)
        def _():
            for copy in o_copies(i):
                copy.start()
        return carry
    lax.fori_loop(0, nx, last, 0)

    for i in range(1, nx):
        src = lax.rem(x - i + nx, nx)
        for copy in o_copies(i):
            copy.wait_recv()
    stats = [sb[0]] + [srv[i] for i in range(1, nx)]
    outs = [ob[0]] + [orv[i] for i in range(1, nx)]
    top = functools.reduce(jnp.maximum, stats)
    shares = [jnp.exp2(t - top) for t in stats]
    whole = functools.reduce(jnp.add, shares)
    shares = [t / whole for t in shares]
    merged = [jnp.zeros((128, 256), F32), jnp.zeros((64, 256), F32), jnp.zeros((64, 256), F32)]
    for i in range(nx):
        for h, (first, size) in enumerate(((0, 128), (128, 64), (192, 64))):
            merged[h] = merged[h] + shares[i][h:h + 1] * outs[i][first:first + size].astype(F32)
    ab[...] = jnp.transpose(jnp.concatenate(merged, axis=0)).astype(BF16)

    share = 256 // ny

    def rows_of(y_):
        return ab.at[pl.ds(pl.multiple_of(y_ * share, share), share), :]

    def y_copy(i):
        other = lax.rem(y + i, ny)
        return remote(rows_of(other), ar.at[y], y_s.at[i - 1], y_r.at[i - 1], at(z, x, c, other))

    for i in range(1, ny):
        y_copy(i).start()
    for copy in weights[2:]:
        copy.start()
    ar[y] = ab[pl.ds(pl.multiple_of(y * share, share), share), :]
    for i in range(1, ny):
        src = lax.rem(y - i + ny, ny)
        remote(rows_of(src), ar.at[src], y_s.at[i - 1], y_r.at[i - 1], at(z, x, c, src)).wait_recv()

    for copy in fetch[:2]:
        copy.wait()
    a_wide = jnp.concatenate([ar[k, :, :128] for k in range(ny)], axis=1)
    a_narrow = jnp.concatenate([ar[k, :, 128:] for k in range(ny)], axis=1)
    mixed = jnp.dot(a_wide, ow[...], preferred_element_type=F32) + jnp.dot(a_narrow, on[...], preferred_element_type=F32)
    middle = (res_ref[...].astype(F32) + mixed).astype(BF16)
    mid[...] = middle
    middle = middle.astype(F32)
    spread = jnp.mean(middle * middle, axis=1, keepdims=True)
    normed = (middle * lax.rsqrt(spread + epsilon) * gain_ref[...]).astype(BF16)
    picker = jnp.where(chosen[0] | chosen[1], 1.0, 0.0).astype(BF16)
    perm[...] = lax.dot_general(picker, normed, (((0,), (0,)), ((), ())), preferred_element_type=F32)

    def cut(k, carry):
        v = perm[pl.ds(pl.multiple_of(8 * k, 8), 8), :]
        snd[2 * k] = v[:4].astype(BF16)
        snd[2 * k + 1] = v[4:].astype(BF16)
        return carry
    lax.fori_loop(0, count // 2, cut, 0)

    def to_plane(t):
        return lax.rem(z + far_first(t, nz) + nz, nz)

    def from_plane(t):
        return lax.rem(z - far_first(t, nz) + nz, nz)

    def out_copy(e):
        return remote(snd.at[e], arr.at[sp], a_s.at[e], a_r.at[sp], (e, y))

    def each_other(p, act):
        def one(k, carry):
            e = p * plane + k

            @pl.when(e != sp)
            def _():
                act(e)
            return carry
        lax.fori_loop(0, plane, one, 0)

    def send_rows(t, carry):
        each_other(to_plane(t), lambda e: out_copy(e).start())
        return carry
    lax.fori_loop(0, nz, send_rows, 0)
    keep = pltpu.make_async_copy(snd.at[sp], arr.at[sp], loc2.at[5])
    keep.start()
    keep.wait()

    def to_rows(take):
        for k in range(plane // 2):
            tmp[8 * k:8 * k + 8, :] = jnp.concatenate([take(2 * k).astype(F32), take(2 * k + 1).astype(F32)], axis=0)

    def rows_at(t):
        return pl.ds(pl.multiple_of(t * step, step), step)

    def cross_copy(p):
        some = pl.ds(p * plane, plane)
        return remote(arr.at[some], arc.at[some], c_s.at[p], c_r.at[p], across)

    def arrive_cross(t):
        p = from_plane(t)
        cross_copy(p).wait_recv()
        to_rows(lambda k: arc[p * plane + k])
        xs[rows_at(t), :] = tmp[...].astype(BF16)

    def arrive(t, carry):
        p = from_plane(t)
        each_other(p, lambda s: remote(snd.at[s], arr.at[s], a_s.at[s], a_r.at[s], (s, y)).wait_recv())
        cross_copy(p).start()
        to_rows(lambda k: arr[p * plane + k])
        xo[rows_at(t), :] = tmp[...].astype(BF16)

        @pl.when(t >= nz // 2)
        def _():
            arrive_cross(t - nz // 2)
        return carry
    lax.fori_loop(0, nz, arrive, 0)
    for copy in fetch[2:]:
        copy.wait()
    for copy in weights:
        copy.wait_recv()

    def hidden(x):
        both = []
        for k in range(2):
            g = jnp.dot(x, wg[k], preferred_element_type=F32)
            u = jnp.dot(x, wu[k], preferred_element_type=F32)
            both.append((jax.nn.silu(g) * u).astype(BF16))
        return both

    def down(h, put):
        width = 512
        for q in range(wd.shape[2] // width):
            cols = slice(q * width, (q + 1) * width)
            put(
                cols,
                jnp.dot(h[0], wd[0, :, cols], preferred_element_type=F32)
                + jnp.dot(h[1], wd[1, :, cols], preferred_element_type=F32),
            )

    def part_copy(t):
        some = rows_at(t)
        return remote(part.at[some, :], back.at[some, :], p_s.at[t], p_r.at[t], across)

    def send_part(t, carry):
        part_copy(t).start()
        return carry

    def cross_half(k):
        some = slice(k * step * nz // 2, (k + 1) * step * nz // 2)

        def put(cols, value):
            part[some, cols] = value.astype(BF16)
        down(hidden(xs[some, :]), put)
        lax.fori_loop(k * nz // 2, (k + 1) * nz // 2, send_part, 0)

    cross_half(0)

    def put_total(cols, value):
        total[:, cols] = value
    down(hidden(xo[...]), put_total)

    def late(t, carry):
        arrive_cross(t)
        return carry
    lax.fori_loop(nz // 2, nz, late, 0)
    cross_half(1)

    def back_copy(e):
        return remote(bsd.at[e], ret.at[sp], b_s.at[e], b_r.at[sp], (e, y))

    def finish(t, carry):
        p = from_plane(t)
        part_copy(t).wait_recv()
        some = rows_at(t)
        tmp[...] = total[some, :] + back[some, :].astype(F32)
        for k in range(plane // 2):
            v = tmp[8 * k:8 * k + 8, :]
            bsd[p * plane + 2 * k] = v[:4].astype(BF16)
            bsd[p * plane + 2 * k + 1] = v[4:].astype(BF16)
        each_other(p, lambda e: back_copy(e).start())
        return carry
    lax.fori_loop(0, nz, finish, 0)
    last = pltpu.make_async_copy(bsd.at[sp], ret.at[sp], loc2.at[6])
    last.start()
    last.wait()

    def returned(t, carry):
        p = to_plane(t)
        each_other(p, lambda e: remote(bsd.at[e], ret.at[e], b_s.at[e], b_r.at[e], (e, y)).wait_recv())
        to_rows(lambda k: ret[p * plane + k])
        rows[rows_at(p), :] = tmp[...].astype(BF16)
        return carry
    lax.fori_loop(0, nz, returned, 0)
    mix = jnp.where(chosen[0], weight_ref[:, 0:1], 0.0) + jnp.where(chosen[1], weight_ref[:, 1:2], 0.0)
    combined = mid[...].astype(F32)
    for _ in range(3):
        term = mix.astype(BF16)
        mix = mix - term.astype(F32)
        combined = combined + jnp.dot(term, rows[...], preferred_element_type=F32)
    out_ref[...] = combined.astype(BF16)

    for copy in weights:
        copy.wait_send()

    def drain(t, carry):
        each_other(t, lambda e: out_copy(e).wait_send())
        each_other(t, lambda e: back_copy(e).wait_send())
        cross_copy(t).wait_send()
        part_copy(t).wait_send()
        return carry
    lax.fori_loop(0, nz, drain, 0)
    for j in range(2):
        if up_has(1, j):
            own_up(j).wait_send()
        if dn_has(1, j):
            own_dn(j).wait_send()
        own_pr(j).wait_send()
        for s in range(1, half + 1):
            if up_has(s, j):
                if up_has(s + 1, j):
                    up_copy(s, j).wait_send()
                pr_copy(zdn(s), j).wait_send()
            if dn_has(s, j):
                if dn_has(s + 1, j):
                    dn_copy(s, j).wait_send()
                pr_copy(zup(s), j).wait_send()
    for i in range(1, 2 * nx):
        t1_copy(i).wait_send()
    for i in range(1, nz):
        t2_copy(i).wait_send()
    for i in range(1, nx):
        q_copy(i).wait_send()
        for copy in o_copies(i):
            copy.wait_send()
    for i in range(1, ny):
        y_copy(i).wait_send()


def layer(dims, arrays):
    nz, nx, ny = dims
    half, count = nz // 2, nz * nx * 2
    residual, wide, narrow, gate, up, down = (arrays[i] for i in (0, 9, 10, 14, 15, 16))
    features = residual.shape[1]
    dma = pltpu.SemaphoreType.DMA
    vmem = pl.BlockSpec(memory_space=pltpu.VMEM)
    hbm = pl.BlockSpec(memory_space=pl.ANY)
    blocks = pltpu.VMEM((count, 4, features), BF16)
    table = pltpu.VMEM((4 * count, features), BF16)
    square = pltpu.VMEM((256, 256), BF16)
    return pl.pallas_call(
        functools.partial(layer_kernel, dims),
        out_shape=jax.ShapeDtypeStruct(residual.shape, BF16),
        in_specs=[vmem] * 9 + [hbm] * 2 + [vmem] * 3 + [hbm] * 3,
        out_specs=vmem,
        scratch_shapes=[
            square,
            pltpu.VMEM((288, 256), BF16),
            square,
            pltpu.VMEM((1, 128), F32),
            pltpu.VMEM((nx, 256, 256), BF16),
            pltpu.VMEM((nz, 2, 288, 256), BF16),
            pltpu.VMEM((nz, 2, 256, 256), BF16),
            pltpu.VMEM((nz, 2 * nx, 1, 128), F32),
            pltpu.VMEM((512, 128), BF16),
            pltpu.VMEM((nx, 3, 1, 256), F32),
            pltpu.VMEM((nx, 304, 256), F32),
            pltpu.VMEM((nx, 256, 256), BF16),
            pltpu.VMEM((nx, 8, 256), F32),
            pltpu.VMEM((nx, 256, 256), BF16),
            pltpu.VMEM((nx, 8, 256), F32),
            square,
            pltpu.VMEM((ny, 256 // ny, 256), BF16),
            dma((nx,)), dma((nx,)),
            dma((half + 1, 2)), dma((half + 1, 2)), dma((half + 1, 2)), dma((half + 1, 2)),
            dma((nz, 2)), dma((nz, 2)),
            dma((2 * nx,)), dma((2 * nx,)), dma((nz,)), dma((nz,)),
            dma((nx, 2)), dma((nx, 2)), dma((ny,)), dma((ny,)), dma((4,)),
            pltpu.VMEM(wide.shape, BF16),
            pltpu.VMEM(narrow.shape, BF16),
            pltpu.VMEM((4 * count, features), F32),
            pltpu.VMEM((8 * nx, features), F32),
            blocks, blocks, blocks, table, table,
            pltpu.VMEM(residual.shape, BF16),
            pltpu.VMEM((2, *gate.shape), BF16),
            pltpu.VMEM((2, *up.shape), BF16),
            pltpu.VMEM((2, *down.shape), BF16),
            pltpu.VMEM((4 * count, features), F32),
            table, table, blocks, blocks, table,
            dma((count,)), dma((count,)), dma((nz,)), dma((nz,)), dma((nz,)), dma((nz,)),
            dma((count,)), dma((count,)), dma((4,)), dma((4,)), dma((7,)),
        ],
        compiler_params=pltpu.CompilerParams(collective_id=1, has_side_effects=True, vmem_limit_bytes=60 * 2**20),
        cost_estimate=pl.CostEstimate(flops=10**10, bytes_accessed=10**7, transcendentals=10**7),
        name="layer",
    )(*arrays)


def body(
    residual,
    query_wide,
    key_wide,
    value_wide,
    query_narrow,
    key_narrow,
    value_narrow,
    gate_wide,
    gate_narrow,
    out_wide,
    out_narrow,
    norm_gain,
    routing,
    route_weight,
    gate_weight,
    up_weight,
    down_weight,
):
    ny = lax.axis_size("tp")
    nx = NX
    dims = (lax.axis_size("sp") // (2 * nx), nx, ny)
    gate, up, down = gate_weight[0], up_weight[0], down_weight[0]
    return layer(
        dims,
        (
            residual, query_wide, key_wide, value_wide, query_narrow, key_narrow, value_narrow, gate_wide, gate_narrow,
            out_wide, out_narrow, norm_gain[None, :], routing, route_weight, gate, up, down,
        ),
    )


def solution(mesh):
    placed = (
        P(("sp", "tp"), None),
        P("sp", "tp"),
        P("sp", "tp"),
        P("sp", "tp"),
        P("sp", "tp"),
        P("sp", "tp"),
        P("sp", "tp"),
        P("sp", "tp"),
        P("sp", "tp"),
        P(),
        P(),
        P(),
        P(("sp", "tp"), None),
        P(("sp", "tp"), None),
        P("sp", None, "tp"),
        P("sp", None, "tp"),
        P("sp", "tp", None),
    )
    return jax.shard_map(
        body, mesh=mesh, in_specs=placed, out_specs=P(("sp", "tp"), None), check_vma=False
    )
```

time: 155 us -> 141 us (0.910)
  Pallas kernels: 140 us -> 133 us
  other arithmetic: 3.64 us -> 0 us
  local copies, waits for them, and re-layouts: 10.8 us -> 7.36 us
    pallas_call x2 -> x1, Pallas kernels: 140 us -> 133 us  [layer(): pl.pallas_call(functools.partial(layer_kernel, dims), out_shape=jax.Shape...]
    unnamed x29 -> x5, local copies, waits for them, and re-layouts: 10.3 us -> 7.36 us
    concatenate x2 -> x0, other arithmetic: 1.86 us -> none  [the longest x1 0.97 us: prepare(): q = jnp.concatenate([query_wide, query_narrow], axis=1)]
where the time goes in v4:
time: 141 us; the launch traced here: 140 us
  Pallas kernels  133 us (94%)
  local copies, waits for them, and re-layouts  7.36 us (5%)
    pallas_call x1, Pallas kernels, layer(): pl.pallas_call(functools.partial(layer_kernel, dims), out_shape=jax.Shape...  133 us
    unnamed x5, local copies, waits for them, and re-layouts  7.36 us

profile of v4, /device:TPU:1, one launch (start us, length us, event | category | flops | bytes accessed | tf_op | source)
XLA Modules:
  0.0 140.5 jit_solution(10203988444119266162)
XLA Ops:
  0.0 1.4 copy.20.routing_ref
  1.4 1.4 copy.21.weight_ref
  2.7 1.5 %copy.18.gw_ref = f32[256,1]{1,0:T(8,128)} copy(f32[256,1]{0,1:T(1,128)} %param.24) | data formatting | bytes 2048 | tf_op args[7]
  4.2 1.5 %copy.19.gn_ref = f32[256,2]{1,0:T(8,128)} copy(f32[256,2]{0,1:T(2,128)} %param.25) | data formatting | bytes 4096 | tf_op args[8]
  5.7 133.1 %layer.1 = bf16[64,2048]{1,0:T(8,128)(2,1)} custom-call(bf16[64,2048]{1,0:T(8,128)(2,1)} %res_ref.1, bf16[256,128]{1,0:T(8,128)(2,1)} %qw_ref.1, bf16[256,128]{1,0:T(8,128)(2,1)} %kw_ref.1, bf16[256,128]{1,0:T(8,128)(2,1)} %vw_ref.1, bf16[256,128]{1,0:T(8,128)(2,1)} %qn_ref.1, bf16[256,128]{1,0:T(8,128)(2,1)} %kn_ref.1, bf16[256,128]{1,0:T(8,128)(2,1)} %vn_ref.1, ...), custom_call_target="tpu_custom_call" | custom-call | flops 10000000000 | bytes 10000000 | tf_op jit(solution)/shard_map/layer/pallas_call | solution.py:617
  138.8 1.7 %copy.23 = bf16[64,2048]{1,0:T(8,128)(2,1)} copy(bf16[64,2048]{1,0:T(8,128)(2,1)} %layer.1) | data formatting | bytes 524288

commit v5 on v4

--- a/solution.py
+++ b/solution.py
@@ -23,8 +23,8 @@
     return lax.rem(y, 2) * (y - 1) + (1 - lax.rem(y, 2)) * (y + 1)
 
 
-def far_first(t, nz):
-    m = nz // 2 - (t + 1) // 2
+def near_first(t, nz):
+    m = (t + 1) // 2
     return jnp.where((lax.rem(t, 2) == 0) & (t > 0), -m, m)
 
 
@@ -34,7 +34,7 @@
     q_ref, kd_ref, v_ref, tot_ref, qb, kb, vb, tt, kaug, mb, acc, ob, sb, orv, srv, ab, ar,
     q_s, q_r, up_s, up_r, dn_s, dn_r, pr_s, pr_r, t1_s, t1_r, t2_s, t2_r, o_s, o_r, y_s, y_r, loc,
     ow, on, perm, tmp, snd, arr, arc, xo, xs, mid, wg, wu, wd, total, part, back, bsd, ret, rows,
-    a_s, a_r, c_s, c_r, p_s, p_r, b_s, b_r, w_s, w_r, loc2,
+    a_s, a_r, c_s, c_r, p_s, p_r, b_s, b_r, w_s, w_r, loc2, vw_in, vn_in, qw_in, qn_in, res_in,
 ):
     nz, nx, ny = dims
     half = nz // 2
@@ -42,7 +42,18 @@
     count = nz * plane
     step = 4 * plane
     sp, y = lax.axis_index("sp"), lax.axis_index("tp")
+    early_in = [
+        pltpu.make_async_copy(kw_ref, kd_ref.at[pl.ds(0, 256), pl.ds(0, 128)], loc2.at[7]),
+        pltpu.make_async_copy(kn_ref, kd_ref.at[pl.ds(0, 256), pl.ds(128, 128)], loc2.at[8]),
+        pltpu.make_async_copy(vw_ref, vw_in, loc2.at[9]),
+        pltpu.make_async_copy(vn_ref, vn_in, loc2.at[10]),
+        pltpu.make_async_copy(qw_ref, qw_in, loc2.at[11]),
+        pltpu.make_async_copy(qn_ref, qn_in, loc2.at[12]),
+    ]
+    for copy in early_in:
+        copy.start()
     fetch = [
+        pltpu.make_async_copy(res_ref, res_in, loc2.at[13]),
         pltpu.make_async_copy(wide_ref, ow, loc2.at[0]),
         pltpu.make_async_copy(narrow_ref, on, loc2.at[1]),
         pltpu.make_async_copy(gate_ref, wg.at[0], loc2.at[2]),
@@ -86,44 +97,44 @@
     for i in range(1, ny):
         greet((sp, lax.rem(y + i, ny)))
     lane = lax.broadcasted_iota(jnp.int32, (1, 128), 1)
-    gates = jnp.where(lane == 0, gw_ref[...], jnp.where(lane == 1, gn_ref[:, 0:1], gn_ref[:, 1:2]))
+    head = lax.broadcasted_iota(jnp.int32, (8, 1), 0)
+    gates = jnp.where(head == 0, gw_ref[...], jnp.where(head == 1, gn_ref[0:1, :], gn_ref[1:2, :]))
     logs = jnp.minimum(gates, 0.0) - jnp.log1p(jnp.exp(-jnp.abs(gates)))
-    logs = jnp.where(lane < 3, logs, 0.0)
-    until = lax.broadcasted_iota(jnp.int32, (256, 256), 1) <= lax.broadcasted_iota(jnp.int32, (256, 256), 0)
+    until = lax.broadcasted_iota(jnp.int32, (256, 256), 0) <= lax.broadcasted_iota(jnp.int32, (256, 256), 1)
     until = jnp.where(until, 1.0, 0.0).astype(BF16)
-    run = jnp.zeros((256, 128), F32)
+    run = jnp.zeros((8, 256), F32)
     for _ in range(3):
         term = logs.astype(BF16)
         logs = logs - term.astype(F32)
-        run = run + jnp.dot(until, term, preferred_element_type=F32)
-    run = run * LOG2E
-    tot_ref[...] = run[255:256]
-    left = jnp.transpose(run)[:8]
+        run = run + jnp.dot(term, until, preferred_element_type=F32)
+    left = run * LOG2E
+    ends = left[:, 255:256]
+    tot_ref[...] = jnp.where(lane == 0, ends[0:1], jnp.where(lane == 1, ends[1:2], ends[2:3]))
     terms = []
     for _ in range(3):
         term = left.astype(BF16).astype(F32)
         left = left - term
         terms.append(term)
     kd_ref[256:288, :] = jnp.concatenate(terms + [jnp.zeros((8, 256), F32)], axis=0).astype(BF16)
-    kd_ref[0:256, :128] = kw_ref[...]
-    kd_ref[0:256, 128:] = kn_ref[...]
-    v_ref[0:128, :] = jnp.transpose(vw_ref[...].astype(F32)).astype(BF16)
-    v_ref[128:256, :] = jnp.transpose(vn_ref[...].astype(F32)).astype(BF16)
-    q_ref[0:128, :] = jnp.transpose(qw_ref[...].astype(F32) * (HW ** -0.5 * LOG2E)).astype(BF16)
-    q_ref[128:256, :] = jnp.transpose(qn_ref[...].astype(F32) * (HN ** -0.5 * LOG2E)).astype(BF16)
-    own_rows = routing_ref.shape[0]
-    names = [routing_ref[:, k:k + 1].astype(F32) for k in range(2)]
-    expert = lax.broadcasted_iota(jnp.int32, (own_rows, count), 1).astype(F32)
+    for copy in early_in:
+        copy.wait()
+    v_ref[0:128, :] = jnp.transpose(vw_in[...].astype(F32)).astype(BF16)
+    v_ref[128:256, :] = jnp.transpose(vn_in[...].astype(F32)).astype(BF16)
+    q_ref[0:128, :] = jnp.transpose(qw_in[...].astype(F32) * (HW ** -0.5 * LOG2E)).astype(BF16)
+    q_ref[128:256, :] = jnp.transpose(qn_in[...].astype(F32) * (HN ** -0.5 * LOG2E)).astype(BF16)
+    own_rows = routing_ref.shape[1]
+    names = [routing_ref[k:k + 1, :].astype(F32) for k in range(2)]
+    expert = lax.broadcasted_iota(jnp.int32, (count, own_rows), 0).astype(F32)
     hits = [jnp.where(name == expert, 1.0, 0.0) for name in names]
-    earlier = lax.broadcasted_iota(jnp.int32, (own_rows, own_rows), 1) < lax.broadcasted_iota(
-        jnp.int32, (own_rows, own_rows), 0
+    earlier = lax.broadcasted_iota(jnp.int32, (own_rows, own_rows), 0) < lax.broadcasted_iota(
+        jnp.int32, (own_rows, own_rows), 1
     )
     before = jnp.dot(
-        jnp.where(earlier, 1.0, 0.0).astype(BF16), (hits[0] + hits[1]).astype(BF16), preferred_element_type=F32
+        (hits[0] + hits[1]).astype(BF16), jnp.where(earlier, 1.0, 0.0).astype(BF16), preferred_element_type=F32
     )
-    slot = lax.broadcasted_iota(jnp.int32, (own_rows, 4 * count), 1).astype(F32)
+    slot = lax.broadcasted_iota(jnp.int32, (4 * count, own_rows), 0).astype(F32)
     chosen = [
-        slot == names[k] * 4.0 + jnp.sum(before * hits[k], axis=1, keepdims=True) for k in range(2)
+        slot == names[k] * 4.0 + jnp.sum(before * hits[k], axis=0, keepdims=True) for k in range(2)
     ]
     pl.semaphore_wait(barrier, count - 1 + ny - 1)
 
@@ -405,18 +416,18 @@
         src = lax.rem(y - i + ny, ny)
         remote(rows_of(src), ar.at[src], y_s.at[i - 1], y_r.at[i - 1], at(z, x, c, src)).wait_recv()
 
-    for copy in fetch[:2]:
+    for copy in fetch[:3]:
         copy.wait()
     a_wide = jnp.concatenate([ar[k, :, :128] for k in range(ny)], axis=1)
     a_narrow = jnp.concatenate([ar[k, :, 128:] for k in range(ny)], axis=1)
     mixed = jnp.dot(a_wide, ow[...], preferred_element_type=F32) + jnp.dot(a_narrow, on[...], preferred_element_type=F32)
-    middle = (res_ref[...].astype(F32) + mixed).astype(BF16)
+    middle = (res_in[...].astype(F32) + mixed).astype(BF16)
     mid[...] = middle
     middle = middle.astype(F32)
     spread = jnp.mean(middle * middle, axis=1, keepdims=True)
     normed = (middle * lax.rsqrt(spread + epsilon) * gain_ref[...]).astype(BF16)
     picker = jnp.where(chosen[0] | chosen[1], 1.0, 0.0).astype(BF16)
-    perm[...] = lax.dot_general(picker, normed, (((0,), (0,)), ((), ())), preferred_element_type=F32)
+    perm[...] = jnp.dot(picker, normed, preferred_element_type=F32)
 
     def cut(k, carry):
         v = perm[pl.ds(pl.multiple_of(8 * k, 8), 8), :]
@@ -426,10 +437,10 @@
     lax.fori_loop(0, count // 2, cut, 0)
 
     def to_plane(t):
-        return lax.rem(z + far_first(t, nz) + nz, nz)
+        return lax.rem(z + near_first(t, nz) + nz, nz)
 
     def from_plane(t):
-        return lax.rem(z - far_first(t, nz) + nz, nz)
+        return lax.rem(z - near_first(t, nz) + nz, nz)
 
     def out_copy(e):
         return remote(snd.at[e], arr.at[sp], a_s.at[e], a_r.at[sp], (e, y))
@@ -481,7 +492,7 @@
             arrive_cross(t - nz // 2)
         return carry
     lax.fori_loop(0, nz, arrive, 0)
-    for copy in fetch[2:]:
+    for copy in fetch[3:]:
         copy.wait()
     for copy in weights:
         copy.wait_recv()
@@ -509,7 +520,7 @@
         return remote(part.at[some, :], back.at[some, :], p_s.at[t], p_r.at[t], across)
 
     def send_part(t, carry):
-        part_copy(t).start()
+        part_copy(nz - 1 - t).start()
         return carry
 
     def cross_half(k):
@@ -518,64 +529,30 @@
         def put(cols, value):
             part[some, cols] = value.astype(BF16)
         down(hidden(xs[some, :]), put)
-        lax.fori_loop(k * nz // 2, (k + 1) * nz // 2, send_part, 0)
-
-    cross_half(0)
 
     def put_total(cols, value):
         total[:, cols] = value
     down(hidden(xo[...]), put_total)
+    cross_half(0)
 
     def late(t, carry):
         arrive_cross(t)
         return carry
     lax.fori_loop(nz // 2, nz, late, 0)
     cross_half(1)
+    lax.fori_loop(0, nz, send_part, 0)
 
     def back_copy(e):
         return remote(bsd.at[e], ret.at[sp], b_s.at[e], b_r.at[sp], (e, y))
 
-    def finish(t, carry):
-        p = from_plane(t)
-        part_copy(t).wait_recv()
-        some = rows_at(t)
-        tmp[...] = total[some, :] + back[some, :].astype(F32)
-        for k in range(plane // 2):
-            v = tmp[8 * k:8 * k + 8, :]
-            bsd[p * plane + 2 * k] = v[:4].astype(BF16)
-            bsd[p * plane + 2 * k + 1] = v[4:].astype(BF16)
-        each_other(p, lambda e: back_copy(e).start())
-        return carry
-    lax.fori_loop(0, nz, finish, 0)
-    last = pltpu.make_async_copy(bsd.at[sp], ret.at[sp], loc2.at[6])
-    last.start()
-    last.wait()
-
-    def returned(t, carry):
-        p = to_plane(t)
-        each_other(p, lambda e: remote(bsd.at[e], ret.at[e], b_s.at[e], b_r.at[e], (e, y)).wait_recv())
-        to_rows(lambda k: ret[p * plane + k])
-        rows[rows_at(p), :] = tmp[...].astype(BF16)
-        return carry
-    lax.fori_loop(0, nz, returned, 0)
-    mix = jnp.where(chosen[0], weight_ref[:, 0:1], 0.0) + jnp.where(chosen[1], weight_ref[:, 1:2], 0.0)
-    combined = mid[...].astype(F32)
-    for _ in range(3):
-        term = mix.astype(BF16)
-        mix = mix - term.astype(F32)
-        combined = combined + jnp.dot(term, rows[...], preferred_element_type=F32)
-    out_ref[...] = combined.astype(BF16)
-
     for copy in weights:
         copy.wait_send()
 
-    def drain(t, carry):
+    def drain_rows(t, carry):
         each_other(t, lambda e: out_copy(e).wait_send())
-        each_other(t, lambda e: back_copy(e).wait_send())
         cross_copy(t).wait_send()
-        part_copy(t).wait_send()
-        return carry
-    lax.fori_loop(0, nz, drain, 0)
+        return carry
+    lax.fori_loop(0, nz, drain_rows, 0)
     for j in range(2):
         if up_has(1, j):
             own_up(j).wait_send()
@@ -602,6 +579,46 @@
     for i in range(1, ny):
         y_copy(i).wait_send()
 
+    def finish(u, carry):
+        t = nz - 1 - u
+        p = from_plane(t)
+        part_copy(t).wait_recv()
+        some = rows_at(t)
+        tmp[...] = total[some, :] + back[some, :].astype(F32)
+        for k in range(plane // 2):
+            v = tmp[8 * k:8 * k + 8, :]
+            bsd[p * plane + 2 * k] = v[:4].astype(BF16)
+            bsd[p * plane + 2 * k + 1] = v[4:].astype(BF16)
+        each_other(p, lambda e: back_copy(e).start())
+        return carry
+    lax.fori_loop(0, nz, finish, 0)
+    last = pltpu.make_async_copy(bsd.at[sp], ret.at[sp], loc2.at[6])
+    last.start()
+    last.wait()
+
+    def returned(u, carry):
+        p = to_plane(nz - 1 - u)
+        each_other(p, lambda e: remote(bsd.at[e], ret.at[e], b_s.at[e], b_r.at[e], (e, y)).wait_recv())
+        to_rows(lambda k: ret[p * plane + k])
+        rows[rows_at(p), :] = tmp[...].astype(BF16)
+        return carry
+    lax.fori_loop(0, nz, returned, 0)
+    mix = jnp.where(chosen[0], weight_ref[0:1, :], 0.0) + jnp.where(chosen[1], weight_ref[1:2, :], 0.0)
+    combined = mid[...].astype(F32)
+    for _ in range(3):
+        term = mix.astype(BF16)
+        mix = mix - term.astype(F32)
+        combined = combined + lax.dot_general(
+            term, rows[...], (((0,), (0,)), ((), ())), preferred_element_type=F32
+        )
+    out_ref[...] = combined.astype(BF16)
+
+    def drain(t, carry):
+        each_other(t, lambda e: back_copy(e).wait_send())
+        part_copy(t).wait_send()
+        return carry
+    lax.fori_loop(0, nz, drain, 0)
+
 
 def layer(dims, arrays):
     nz, nx, ny = dims
@@ -617,7 +634,7 @@
     return pl.pallas_call(
         functools.partial(layer_kernel, dims),
         out_shape=jax.ShapeDtypeStruct(residual.shape, BF16),
-        in_specs=[vmem] * 9 + [hbm] * 2 + [vmem] * 3 + [hbm] * 3,
+        in_specs=[hbm] * 7 + [vmem] * 2 + [hbm] * 2 + [vmem] * 3 + [hbm] * 3,
         out_specs=vmem,
         scratch_shapes=[
             square,
@@ -654,7 +671,9 @@
             pltpu.VMEM((4 * count, features), F32),
             table, table, blocks, blocks, table,
             dma((count,)), dma((count,)), dma((nz,)), dma((nz,)), dma((nz,)), dma((nz,)),
-            dma((count,)), dma((count,)), dma((4,)), dma((4,)), dma((7,)),
+            dma((count,)), dma((count,)), dma((4,)), dma((4,)), dma((14,)),
+            pltpu.VMEM((256, 128), BF16), pltpu.VMEM((256, 128), BF16), pltpu.VMEM((256, 128), BF16), pltpu.VMEM((256, 128), BF16),
+            pltpu.VMEM(residual.shape, BF16),
         ],
         compiler_params=pltpu.CompilerParams(collective_id=1, has_side_effects=True, vmem_limit_bytes=60 * 2**20),
         cost_estimate=pl.CostEstimate(flops=10**10, bytes_accessed=10**7, transcendentals=10**7),
@@ -688,8 +707,8 @@
     return layer(
         dims,
         (
-            residual, query_wide, key_wide, value_wide, query_narrow, key_narrow, value_narrow, gate_wide, gate_narrow,
-            out_wide, out_narrow, norm_gain[None, :], routing, route_weight, gate, up, down,
+            residual, query_wide, key_wide, value_wide, query_narrow, key_narrow, value_narrow, gate_wide.T, gate_narrow.T,
+            out_wide, out_narrow, norm_gain[None, :], routing.T, route_weight.T, gate, up, down,
         ),
     )
 

time: 141 us -> 132 us (0.936)
  local copies, waits for them, and re-layouts: 7.36 us -> 1.67 us
  Pallas kernels: 133 us -> 130 us
    unnamed x5 -> x1, local copies, waits for them, and re-layouts: 7.36 us -> 1.67 us
    pallas_call x1, Pallas kernels: 133 us -> 130 us  [layer(): pl.pallas_call(functools.partial(layer_kernel, dims), out_shape=jax.Shape...]
where the time goes in v5:
time: 132 us
  Pallas kernels  130 us (98%)
  local copies, waits for them, and re-layouts  1.67 us (1%)
    pallas_call x1, Pallas kernels, layer(): pl.pallas_call(functools.partial(layer_kernel, dims), out_shape=jax.Shape...  130 us

profile of v5, /device:TPU:1, one launch (start us, length us, event | category | flops | bytes accessed | tf_op | source)
XLA Modules:
  0.0 131.6 jit_solution(14715720518029257354)
XLA Ops:
  0.0 129.9 %layer.1 = bf16[64,2048]{1,0:T(8,128)(2,1)} custom-call(bf16[64,2048]{1,0:T(8,128)(2,1)} %res_ref.1, bf16[256,128]{1,0:T(8,128)(2,1)} %qw_ref.1, bf16[256,128]{1,0:T(8,128)(2,1)} %kw_ref.1, bf16[256,128]{1,0:T(8,128)(2,1)} %vw_ref.1, bf16[256,128]{1,0:T(8,128)(2,1)} %qn_ref.1, bf16[256,128]{1,0:T(8,128)(2,1)} %kn_ref.1, bf16[256,128]{1,0:T(8,128)(2,1)} %vn_ref.1, ...), custom_call_target="tpu_custom_call" | custom-call | flops 10000000000 | bytes 10000000 | tf_op jit(solution)/shard_map/layer/pallas_call | solution.py:634
  129.9 1.7 %copy.19 = bf16[64,2048]{1,0:T(8,128)(2,1)} copy(bf16[64,2048]{1,0:T(8,128)(2,1)} %layer.1) | data formatting | bytes 524288

commit v6 on v5

--- a/solution.py
+++ b/solution.py
@@ -24,8 +24,23 @@
 
 
 def near_first(t, nz):
-    m = (t + 1) // 2
-    return jnp.where((lax.rem(t, 2) == 0) & (t > 0), -m, m)
+    near = nz // 4 * 2
+    u = t - jnp.where(t > near, 1, 0)
+    m = u // 2 + 1
+    return jnp.where(t == near, 0, jnp.where(lax.rem(u, 2) == 0, m, -m))
+
+
+def return_order(nz):
+    if nz == 8:
+        return (2, 3, 7, 6, 5, 0, 1, 4), 2
+    return tuple(range(nz - 1, -1, -1)), 0
+
+
+def entry(table, u):
+    value = 0
+    for i, v in enumerate(table):
+        value = jnp.where(u == i, v, value)
+    return value
 
 
 def layer_kernel(
@@ -115,7 +130,12 @@
         term = left.astype(BF16).astype(F32)
         left = left - term
         terms.append(term)
-    kd_ref[256:288, :] = jnp.concatenate(terms + [jnp.zeros((8, 256), F32)], axis=0).astype(BF16)
+    extra = lax.broadcasted_iota(jnp.int32, (16, 1), 0)
+    placed = jnp.zeros((16, 256), F32)
+    for i in range(3):
+        for h in range(3):
+            placed = jnp.where(extra == 3 * i + h, terms[i][h:h + 1], placed)
+    kd_ref[256:272, :] = placed.astype(BF16)
     for copy in early_in:
         copy.wait()
     v_ref[0:128, :] = jnp.transpose(vw_in[...].astype(F32)).astype(BF16)
@@ -267,19 +287,19 @@
 
     def make_kaug(zb):
         for k in range(2):
-            part = jnp.concatenate([kb[zb, k, 256:288, :].astype(F32), jnp.zeros((96, 256), F32)], axis=0)
+            part = jnp.concatenate([kb[zb, k, 256:272, :].astype(F32), jnp.zeros((112, 256), F32)], axis=0)
             kaug[256 * k:256 * k + 256, :] = jnp.transpose(part).astype(BF16)
 
     spans = ((0, 128), (144, 64), (224, 64))
     row_of = lax.broadcasted_iota(jnp.int32, (128, 256), 0)
-    minus = [jnp.where((lax.rem(row_of, 8) == h) & (row_of < 24), -1.0, 0.0).astype(BF16) for h in range(3)]
-
-    def tiles(zb, offs, masked):
+    minus = [jnp.where((lax.rem(row_of, 3) == h) & (row_of < 9), -1.0, 0.0).astype(BF16) for h in range(3)]
+
+    def tiles(zb, offs, masked, blocks):
         keys = jnp.concatenate([kb[zb, 0, 0:256, :], kb[zb, 1, 0:256, :]], axis=0)
         vals = jnp.concatenate([vb[zb, 0], vb[zb, 1]], axis=1)
         more = kaug[...]
         ones = jnp.ones((16, 512), BF16)
-        work = [(xq, h) for xq in range(nx) for h in range(3)]
+        work = [(xq, h) for xq in blocks for h in range(3)]
         scores, weights_, shrinks = [], [], []
         for xq, h in work:
             side = slice(0, 128) if h == 0 else slice(128, 256)
@@ -317,7 +337,7 @@
 
     def both(zb):
         make_kaug(zb)
-        tiles(zb, offsets(zb), False)
+        tiles(zb, offsets(zb), False, range(nx))
 
     relay(jnp.int32(1))
     for i in range(1, nx):
@@ -329,28 +349,31 @@
     for j in range(2):
         pr_wait(z, j)
     make_kaug(z)
-    tiles(z, offsets(z), True)
+    tiles(z, offsets(z), True, range(nx))
 
     def one_step(s, carry):
+        for j in range(2):
+            pr_wait(zdn(s), j)
+
+        @pl.when(z >= s)
+        def _():
+            both(zdn(s))
+
         @pl.when(s < half)
         def _():
             relay(s + 1)
-        for j in range(2):
-            pr_wait(zdn(s), j)
-
-            @pl.when(s < half)
-            def _():
+            for j in range(2):
                 pr_wait(zup(s), j)
 
-        def side(w, inner):
-            zb = jnp.where(w == 0, zdn(s), zup(s))
-
-            @pl.when(((w == 0) & (z >= s)) | ((w == 1) & (z + s >= nz) & (s < half)))
-            def _():
-                both(zb)
-            return inner
-        return lax.fori_loop(0, 2, side, carry)
-    lax.fori_loop(1, half + 1, one_step, 0)
+        @pl.when((z + s >= nz) & (s < half))
+        def _():
+            both(zup(s))
+        return carry
+    lax.fori_loop(1, half, one_step, 0)
+    for j in range(2):
+        pr_wait(zdn(half), j)
+    make_kaug(zdn(half))
+    last_offs = offsets(zdn(half))
 
     def o_copies(i):
         dev = at(z, lax.rem(x + i, nx), c, y)
@@ -359,10 +382,8 @@
             remote(sb.at[i], srv.at[i], o_s.at[i, 1], o_r.at[i, 1], dev),
         )
 
-    def last(k, carry):
-        i = lax.rem(k + 1, nx)
+    def finalize(i):
         xq = lax.rem(x + i, nx)
-
         outs, lses = [], []
         for h in range(3):
             first, size = spans[h]
@@ -375,12 +396,17 @@
         place = lax.broadcasted_iota(jnp.int32, (8, 256), 0)
         sb[i] = jnp.where(place == 0, lses[0], jnp.where(place == 1, lses[1], lses[2]))
 
-        @pl.when(i > 0)
-        def _():
+        if i > 0:
             for copy in o_copies(i):
                 copy.start()
-        return carry
-    lax.fori_loop(0, nx, last, 0)
+
+    places_ = [(i + 1) % nx for i in range(nx)]
+    for group in ((places_[:nx // 2], places_[nx // 2:]) if nx > 1 else (places_,)):
+        @pl.when(z >= half)
+        def _():
+            tiles(zdn(half), last_offs, False, [lax.rem(x + i, nx) for i in group])
+        for i in group:
+            finalize(i)
 
     for i in range(1, nx):
         src = lax.rem(x - i + nx, nx)
@@ -519,8 +545,10 @@
         some = rows_at(t)
         return remote(part.at[some, :], back.at[some, :], p_s.at[t], p_r.at[t], across)
 
+    order, ahead = return_order(nz)
+
     def send_part(t, carry):
-        part_copy(nz - 1 - t).start()
+        part_copy(entry(order, t)).start()
         return carry
 
     def cross_half(k):
@@ -534,13 +562,15 @@
         total[:, cols] = value
     down(hidden(xo[...]), put_total)
     cross_half(0)
+    for t in range(ahead):
+        send_part(t, 0)
 
     def late(t, carry):
         arrive_cross(t)
         return carry
     lax.fori_loop(nz // 2, nz, late, 0)
     cross_half(1)
-    lax.fori_loop(0, nz, send_part, 0)
+    lax.fori_loop(ahead, nz, send_part, 0)
 
     def back_copy(e):
         return remote(bsd.at[e], ret.at[sp], b_s.at[e], b_r.at[sp], (e, y))
@@ -580,7 +610,7 @@
         y_copy(i).wait_send()
 
     def finish(u, carry):
-        t = nz - 1 - u
+        t = entry(order, u)
         p = from_plane(t)
         part_copy(t).wait_recv()
         some = rows_at(t)
@@ -597,7 +627,7 @@
     last.wait()
 
     def returned(u, carry):
-        p = to_plane(nz - 1 - u)
+        p = to_plane(entry(order, u))
         each_other(p, lambda e: remote(bsd.at[e], ret.at[e], b_s.at[e], b_r.at[e], (e, y)).wait_recv())
         to_rows(lambda k: ret[p * plane + k])
         rows[rows_at(p), :] = tmp[...].astype(BF16)
@@ -638,11 +668,11 @@
         out_specs=vmem,
         scratch_shapes=[
             square,
-            pltpu.VMEM((288, 256), BF16),
+            pltpu.VMEM((272, 256), BF16),
             square,
             pltpu.VMEM((1, 128), F32),
             pltpu.VMEM((nx, 256, 256), BF16),
-            pltpu.VMEM((nz, 2, 288, 256), BF16),
+            pltpu.VMEM((nz, 2, 272, 256), BF16),
             pltpu.VMEM((nz, 2, 256, 256), BF16),
             pltpu.VMEM((nz, 2 * nx, 1, 128), F32),
             pltpu.VMEM((512, 128), BF16),

time: 132 us -> 129 us (0.977)
  Pallas kernels: 130 us -> 127 us
    pallas_call x1, Pallas kernels: 130 us -> 127 us  [layer(): pl.pallas_call(functools.partial(layer_kernel, dims), out_shape=jax.Shape...]
where the time goes in v6:
time: 129 us
  Pallas kernels  127 us (98%)
  local copies, waits for them, and re-layouts  1.67 us (1%)
    pallas_call x1, Pallas kernels, layer(): pl.pallas_call(functools.partial(layer_kernel, dims), out_shape=jax.Shape...  127 us

profile of v6, /device:TPU:1, one launch (start us, length us, event | category | flops | bytes accessed | tf_op | source)
XLA Modules:
  0.0 129.2 jit_solution(16921419229146124625)
XLA Ops:
  0.0 127.5 %layer.1 = bf16[64,2048]{1,0:T(8,128)(2,1)} custom-call(bf16[64,2048]{1,0:T(8,128)(2,1)} %res_ref.1, bf16[256,128]{1,0:T(8,128)(2,1)} %qw_ref.1, bf16[256,128]{1,0:T(8,128)(2,1)} %kw_ref.1, bf16[256,128]{1,0:T(8,128)(2,1)} %vw_ref.1, bf16[256,128]{1,0:T(8,128)(2,1)} %qn_ref.1, bf16[256,128]{1,0:T(8,128)(2,1)} %kn_ref.1, bf16[256,128]{1,0:T(8,128)(2,1)} %vn_ref.1, ...), custom_call_target="tpu_custom_call" | custom-call | flops 10000000000 | bytes 10000000 | tf_op jit(solution)/shard_map/layer/pallas_call | solution.py:664
  127.5 1.7 %copy.19 = bf16[64,2048]{1,0:T(8,128)(2,1)} copy(bf16[64,2048]{1,0:T(8,128)(2,1)} %layer.1) | data formatting | bytes 524288

commit v7 on v6

--- a/solution.py
+++ b/solution.py
@@ -32,7 +32,7 @@
 
 def return_order(nz):
     if nz == 8:
-        return (2, 3, 7, 6, 5, 0, 1, 4), 2
+        return (2, 3, 0, 7, 6, 5, 1, 4), 3
     return tuple(range(nz - 1, -1, -1)), 0
 
 
@@ -244,8 +244,8 @@
     for copy in local[1:]:
         copy.wait()
 
-    def relay(s):
-        for j in range(2):
+    def relay(s, chunks=(0, 1)):
+        for j in chunks:
             @pl.when(s <= (half if j == 0 else half - 1))
             def _():
                 slot = (kb, vb)[j].at[zdn(s), c]
@@ -348,8 +348,10 @@
         remote(slot, slot, t2_s.at[i - 1], t2_r.at[i - 1], at(zdn(i), x, c, y)).wait_recv()
     for j in range(2):
         pr_wait(z, j)
+    relay(jnp.int32(2), (0,))
     make_kaug(z)
     tiles(z, offsets(z), True, range(nx))
+    relay(jnp.int32(2), (1,))
 
     def one_step(s, carry):
         for j in range(2):
@@ -359,11 +361,11 @@
         def _():
             both(zdn(s))
 
-        @pl.when(s < half)
+        @pl.when((s > 1) & (s < half))
         def _():
             relay(s + 1)
-            for j in range(2):
-                pr_wait(zup(s), j)
+        for j in range(2):
+            pr_wait(zup(s), j)
 
         @pl.when((z + s >= nz) & (s < half))
         def _():
@@ -632,7 +634,14 @@
         to_rows(lambda k: ret[p * plane + k])
         rows[rows_at(p), :] = tmp[...].astype(BF16)
         return carry
-    lax.fori_loop(0, nz, returned, 0)
+    lax.fori_loop(0, nz - 1, returned, 0)
+
+    def drain(t, carry):
+        each_other(t, lambda e: back_copy(e).wait_send())
+        part_copy(t).wait_send()
+        return carry
+    lax.fori_loop(0, nz, drain, 0)
+    returned(nz - 1, 0)
     mix = jnp.where(chosen[0], weight_ref[0:1, :], 0.0) + jnp.where(chosen[1], weight_ref[1:2, :], 0.0)
     combined = mid[...].astype(F32)
     for _ in range(3):
@@ -642,12 +651,6 @@
             term, rows[...], (((0,), (0,)), ((), ())), preferred_element_type=F32
         )
     out_ref[...] = combined.astype(BF16)
-
-    def drain(t, carry):
-        each_other(t, lambda e: back_copy(e).wait_send())
-        part_copy(t).wait_send()
-        return carry
-    lax.fori_loop(0, nz, drain, 0)
 
 
 def layer(dims, arrays):

time: 129 us -> 129 us (level); the launches traced: 129 us -> 128 us
    pallas_call x1, Pallas kernels: 127 us -> 126 us  [layer(): pl.pallas_call(functools.partial(layer_kernel, dims), out_shape=jax.Shape...]
where the time goes in v7:
time: 129 us; the launch traced here: 128 us
  Pallas kernels  126 us (98%)
  local copies, waits for them, and re-layouts  1.67 us (1%)
    pallas_call x1, Pallas kernels, layer(): pl.pallas_call(functools.partial(layer_kernel, dims), out_shape=jax.Shape...  126 us

profile of v7, /device:TPU:1, one launch (start us, length us, event | category | flops | bytes accessed | tf_op | source)
XLA Modules:
  0.0 127.6 jit_solution(1646752051502044233)
XLA Ops:
  0.0 126.0 %layer.1 = bf16[64,2048]{1,0:T(8,128)(2,1)} custom-call(bf16[64,2048]{1,0:T(8,128)(2,1)} %res_ref.1, bf16[256,128]{1,0:T(8,128)(2,1)} %qw_ref.1, bf16[256,128]{1,0:T(8,128)(2,1)} %kw_ref.1, bf16[256,128]{1,0:T(8,128)(2,1)} %vw_ref.1, bf16[256,128]{1,0:T(8,128)(2,1)} %qn_ref.1, bf16[256,128]{1,0:T(8,128)(2,1)} %kn_ref.1, bf16[256,128]{1,0:T(8,128)(2,1)} %vn_ref.1, ...), custom_call_target="tpu_custom_call" | custom-call | flops 10000000000 | bytes 10000000 | tf_op jit(solution)/shard_map/layer/pallas_call | solution.py:667
  126.0 1.7 %copy.19 = bf16[64,2048]{1,0:T(8,128)(2,1)} copy(bf16[64,2048]{1,0:T(8,128)(2,1)} %layer.1) | data formatting | bytes 524288
